TPU v7x, 32 devices: a whole 2x2x4 slice. The times are simulated.
32 devices in a mesh: sp: 4 (over z), tp: 8 (over y, x, core).
Axes of the slice: x: 2, y: 2, z: 4, core: 2. Of those that a mesh axis runs over, the one named last changes fastest.
Arguments:
- latent: bfloat16 [2048, 4096], P(('sp', 'tp')), may hold values from -6 to 6
- context: bfloat16 [512, 4096], P('sp'), may hold values from -6 to 6
- condition: float32 [4096], P('sp'), may hold values from -6 to 6
- context_cond: float32 [4096], P('sp'), may hold values from -6 to 6
- mod_weight: bfloat16 [4096, 12288], P('sp', 'tp'), may hold values from -0.09375 to 0.09375
- norm_gain: float32 [4096], replicated, may hold values from 0.1 to 1.9
- query_weight: bfloat16 [4096, 4096], P(None, 'tp'), may hold values from -0.09375 to 0.09375
- key_weight: bfloat16 [4096, 2048], P(None, 'tp'), may hold values from -0.09375 to 0.09375
- value_weight: bfloat16 [4096, 2048], P(None, 'tp'), may hold values from -0.09375 to 0.09375
- out_weight: bfloat16 [4096, 4096], P(None, 'tp'), may hold values from -0.375 to 0.375
- query_gain: float32 [64], replicated, may hold values from 1.2 to 6
- key_gain: float32 [64], replicated, may hold values from 1.2 to 6
- context_lift: float32 [64], P('tp'), may hold values from 0.5 to 2
Outputs:
- updated: bfloat16 [2048, 4096], P(('sp', 'tp'))
All inputs are finite; a program needn't handle non-finite values.
Results may differ from a plain program's by a relative error of at most 0.0085.
The roundings to bfloat16 on the way count: a program that leaves them out, or rounds other values in their place, can miss the bound.
Values may be sent and summed in bfloat16 or wider, within the bound.
A program may use at most 64 MiB of HBM per device.

v0:
```python
import functools

import jax
import jax.numpy as jnp
from jax import lax
from jax.experimental import pallas as pl
from jax.experimental.pallas import tpu as pltpu
from jax.sharding import PartitionSpec as P

GRID_W = 64
EPS = 1e-06
MESH = pl.DeviceIdType.MESH
ANY = pl.BlockSpec(memory_space=pl.ANY)
VMEM = pl.BlockSpec(memory_space=pltpu.VMEM)
SMEM = pl.BlockSpec(memory_space=pltpu.SMEM)
BF16 = jnp.bfloat16
F32 = jnp.float32


def remote(src, dst, send, recv, index, axis, peer):
    return pltpu.make_async_remote_copy(
        src_ref=src, dst_ref=dst, send_sem=send.at[index], recv_sem=recv.at[index],
        device_id={axis: peer}, device_id_type=MESH,
    )


def greet(peers):
    barrier = pltpu.get_barrier_semaphore()
    for axis, peer in peers:
        pl.semaphore_signal(barrier, inc=1, device_id={axis: peer}, device_id_type=MESH)
    pl.semaphore_wait(barrier, len(peers))


def others(axis, count):
    me = lax.axis_index(axis)
    return [(axis, lax.rem(me + step, count)) for step in range(1, count)]


def gather_sems(count):
    return 13 if count == 8 else max(count - 1, 1)


class Gather:
    def __init__(self, count, own, full, send, recv):
        self.count, self.own, self.full, self.send, self.recv = count, own, full, send, recv
        self.me = lax.axis_index("tp")
        self.half = own.shape[0] // 2
        me = self.me
        if count == 8:
            self.core, self.x, self.y = me % 2, (me // 2) % 2, me // 4
            self.sib = me + 1 - 2 * self.core
            self.step = 1 - 2 * self.core
            self.xn = me + 2 - 4 * self.x
            self.yn = me + 4 - 8 * self.y
            self.dn = self.xn + 4 - 8 * self.y

    def part(self, ref, which):
        return ref if which is None else ref.at[pl.ds(which * self.half, self.half)]

    def copy(self, index):
        me, xn, yn, dn, sib = self.me, self.xn, self.yn, self.dn, self.sib
        origin, half, peer = {
            0: (me, 0, xn), 1: (me, 1, xn), 2: (me, 0, yn), 3: (me, 1, yn), 4: (me, None, sib),
            5: (xn, 1, yn), 6: (yn, 0, xn),
            7: (xn, 0, sib), 8: (xn, 1, sib), 9: (yn, 0, sib), 10: (yn, 1, sib),
            11: (dn, 0, sib), 12: (dn, 1, sib),
        }[index]
        source = self.own if index < 5 else self.full.at[origin]
        return remote(self.part(source, half), self.part(self.full.at[origin], half), self.send, self.recv, index, "tp", peer)

    def wait_recv(self, index):
        xn, yn, dn, sib, step = self.xn, self.yn, self.dn, self.sib, self.step
        origin, half = {
            0: (xn, 0), 1: (xn, 1), 2: (yn, 0), 3: (yn, 1), 4: (sib, None), 5: (dn, 1), 6: (dn, 0),
            7: (xn + step, 0), 8: (xn + step, 1), 9: (yn + step, 0), 10: (yn + step, 1),
            11: (dn + step, 0), 12: (dn + step, 1),
        }[index]
        ref = self.part(self.full.at[origin], half)
        remote(ref, ref, self.send, self.recv, index, "tp", sib).wait_recv()

    def direct(self, step):
        peer = lax.rem(self.me + step, self.count)
        return remote(self.own, self.full.at[self.me], self.send, self.recv, step - 1, "tp", peer)

    def start(self):
        if self.count == 8:
            for index in (1, 2, 4):
                self.copy(index).start()
        else:
            for step in range(1, self.count):
                self.direct(step).start()

    def second(self):
        if self.count == 8:
            for index in (0, 3):
                self.copy(index).start()

    def relay(self):
        if self.count == 8:
            for arrived, then in ((1, (5, 8)), (2, (6, 9))):
                self.wait_recv(arrived)
                for nxt in then:
                    self.copy(nxt).start()

    def before(self, index):
        if self.count != 8:
            @pl.when(index == 0)
            def _():
                for step in range(1, self.count):
                    origin = lax.rem(self.me - step + self.count, self.count)
                    ref = self.full.at[origin]
                    remote(ref, ref, self.send, self.recv, step - 1, "tp", origin).wait_recv()
            return

        @pl.when(index == 0)
        def _():
            self.wait_recv(4)

        @pl.when(index == 1)
        def _():
            for arrived, nxt in ((0, 7), (3, 10)):
                self.wait_recv(arrived)
                self.copy(nxt).start()
            self.wait_recv(7)
            self.wait_recv(8)

        @pl.when(index == 2)
        def _():
            self.wait_recv(9)
            self.wait_recv(10)

        @pl.when(index == 3)
        def _():
            self.wait_recv(5)
            self.copy(12).start()
            self.wait_recv(6)
            self.copy(11).start()
            self.wait_recv(12)
            self.wait_recv(11)

    def chip(self, index):
        if self.count == 8:
            return ((self.y + index // 2) % 2) * 2 + (self.x + index) % 2
        return index

    def finish(self):
        if self.count == 8:
            for index in range(13):
                self.copy(index).wait_send()
        else:
            for step in range(1, self.count):
                self.direct(step).wait_send()


def front_kernel(sp, tp, heads, kv_heads, head, stacked, lat, ctx, cond, mod_weight, gain, cos, sin, q_gain, k_gain, lift, *rest):
    weights, rest = rest[: 1 if stacked else 3], rest[1 if stacked else 3 :]
    (attended, gate, full, normed, wide, mod_wide, parts, partial, total, mod, gsc, shf, gains, q_all, kvs, top, acc,
     send, recv, psend, precv, msend, mrecv, zsend, zrecv, local) = rest
    s, f = lax.axis_index("sp"), lax.axis_index("tp")
    rows, model = lat.shape
    width = wide.shape[2]
    slots = wide.shape[0]
    groups = slots - 2
    tile = 2 * rows
    lat_rows = rows * tp
    keys = kvs.shape[2]
    mcols = partial.shape[1]
    tiles = tp // 2 + 1
    scale = head ** -0.5
    mod_in = pltpu.make_async_copy(mod_weight, mod_wide, local.at[slots + 3])
    mod_in.start()
    copies = []
    if stacked:
        copies.append(pltpu.make_async_copy(weights[0], wide, local.at[0]))
    else:
        for n in range(groups):
            copies.append(pltpu.make_async_copy(weights[0].at[:, n * width : (n + 1) * width], wide.at[n], local.at[n]))
        copies.append(pltpu.make_async_copy(weights[1], wide.at[groups], local.at[groups]))
        copies.append(pltpu.make_async_copy(weights[2], wide.at[groups + 1], local.at[groups + 1]))
    own = pltpu.make_async_copy(lat, full.at[f], local.at[slots])
    ctx_in = [
        pltpu.make_async_copy(ctx.at[pl.ds(n * rows, rows)], full.at[tp + n], local.at[slots + 1 + n]) for n in range(2)
    ]
    greet(others("tp", tp) + others("sp", sp))
    gather = Gather(tp, lat, full, send, recv)
    gather.start()
    for item in ctx_in + [own] + copies[::-1]:
        item.start()
    mod_in.wait()
    first_sum = jnp.dot(cond[...], mod_wide[...], preferred_element_type=F32)
    partial[...] = first_sum
    parts[s] = first_sum
    sends = []
    for step in range(1, sp):
        sends.append(remote(partial, parts.at[s], psend, precv, step - 1, "sp", lax.rem(s + step, sp)))
    for item in sends:
        item.start()
    for n in range(slots):
        row = q_gain[...] * scale if n < groups else k_gain[...]
        gains[n] = jnp.concatenate([row] * (width // head), axis=1) if width > head else row
    for step in range(1, sp):
        origin = lax.rem(s - step + sp, sp)
        remote(parts.at[origin], parts.at[origin], psend, precv, step - 1, "sp", origin).wait_recv()
    summed = parts[0]
    for n in range(1, sp):
        summed = summed + parts[n]
    total[...] = summed
    here = pl.ds(pl.multiple_of(f * mcols, mcols), mcols)
    mod[:, here] = summed
    outs = []
    for step in range(1, tp):
        outs.append(remote(total, mod.at[:, here], msend, mrecv, step - 1, "tp", lax.rem(f + step, tp)))
    for item in outs:
        item.start()
    gather.second()
    top[...] = jnp.full(top.shape, -1e30, F32)
    acc[...] = jnp.zeros(acc.shape, F32)
    for step in range(1, tp):
        origin = lax.rem(f - step + tp, tp)
        ref = mod.at[:, pl.ds(pl.multiple_of(origin * mcols, mcols), mcols)]
        remote(ref, ref, msend, mrecv, step - 1, "tp", origin).wait_recv()
    for r in range(2):
        gsc[r] = gain[...] * (1.0 + mod[r : r + 1, model : 2 * model])
        shf[r] = mod[r : r + 1, :model]
    gate[...] = mod[0:1, 2 * model :]
    gather.relay()
    for item in ctx_in + copies:
        item.wait()
    own.wait()

    ring = sp == 4
    right, left, far = (s + 1) % sp, (s + sp - 1) % sp, (s + 2) % sp

    def tile_first(number):
        if isinstance(number, int):
            return lat_rows if number == 0 else pl.multiple_of(gather.chip(number - 1) * tile, tile)
        chip = jnp.where(number == 0, tp // 2, gather.chip(jnp.maximum(number - 1, 0)))
        return pl.multiple_of(chip * tile, tile)

    def ring_copy(number, index):
        which, origin, peer = {
            0: (0, s, right), 1: (1, s, right), 2: (1, s, left), 3: (0, s, left), 4: (0, left, right), 5: (1, right, left),
        }[index]
        ref = kvs.at[origin, which, pl.ds(tile_first(number), tile)]
        return remote(ref, ref, zsend, zrecv, number * 6 + index, "sp", peer)

    def ring_wait(number, index):
        which, origin = {0: (0, left), 1: (1, left), 2: (1, right), 3: (0, right), 4: (0, far), 5: (1, far)}[index]
        ref = kvs.at[origin, which, pl.ds(tile_first(number), tile)]
        remote(ref, ref, zsend, zrecv, number * 6 + index, "sp", right).wait_recv()

    def forward(number):
        ring_wait(number, 0)
        ring_copy(number, 4).start()
        ring_wait(number, 2)
        ring_copy(number, 5).start()

    def direct(step):
        return remote(kvs.at[s], kvs.at[s], zsend, zrecv, step - 1, "sp", lax.rem(s + step, sp))

    even = lax.broadcasted_iota(jnp.int32, (tile, width), 1) % 2 == 0
    same = (
        lax.broadcasted_iota(jnp.int32, (width, width), 0) // head
        == lax.broadcasted_iota(jnp.int32, (width, width), 1) // head
    )
    ones = jnp.where(same, 1.0, 0.0).astype(BF16)
    by_row = (lax.broadcasted_iota(jnp.int32, (1, 2 * head), 1) % head) // 2 < head // 4
    grid_rows = cos.shape[0] - GRID_W
    part = min(tile, GRID_W)
    step_rows = 16

    def roll(v, by):
        if width % 128 == 0:
            return pltpu.roll(v, by % width, axis=1)
        return jnp.concatenate([v[:, width - by % width :], v[:, : width - by % width]], axis=1)

    def table(ref, first, is_ctx, fill):
        pieces = []
        for k in range(tile // part):
            at = jnp.where(is_ctx == 1, 0, first + k * part)
            row = ref[pl.ds(at // GRID_W, 1), :]
            col = ref[pl.ds(pl.multiple_of(grid_rows + at % GRID_W, 8), part), :]
            pieces.append(jnp.where(by_row, row, col))
        v = jnp.concatenate(pieces, axis=0) if len(pieces) > 1 else pieces[0]
        v = jnp.where(is_ctx == 1, fill, v)
        if width > v.shape[1]:
            return jnp.concatenate([v] * (width // v.shape[1]), axis=1)
        return v[:, :width]

    def one_tile(number, unused):
        @pl.when(number > 0)
        def _():
            gather.before(number - 1)

        is_ctx = jnp.where(number == 0, 1, 0)
        first = tile_first(number)
        base = first // rows

        def norm_rows(j, unused):
            slot = base + (j * step_rows) // rows
            row = pl.multiple_of((j * step_rows) % rows, step_rows)
            v = full[slot, pl.ds(row, step_rows), :].astype(F32)
            inv = lax.rsqrt(jnp.mean(v * v, axis=-1, keepdims=True) + EPS)
            out = v * inv * gsc[is_ctx] + shf[is_ctx]
            normed[pl.ds(pl.multiple_of(j * step_rows, step_rows), step_rows), :] = out.astype(BF16)
            return unused

        lax.fori_loop(0, tile // step_rows, norm_rows, 0)

        def turned(y, n):
            sq = y * y
            hi = sq.astype(BF16)
            lo = (sq - hi.astype(F32)).astype(BF16)
            mean = jnp.dot(hi, ones, preferred_element_type=F32) + jnp.dot(lo, ones, preferred_element_type=F32)
            u = y * lax.rsqrt(mean * (1.0 / head) + EPS) * gains[n]
            other = jnp.where(even, roll(u, -1), roll(u, 1))
            return (u * table(cos, first, is_ctx, 1.0) + other * table(sin, first, is_ctx, 0.0)).astype(BF16)

        def one_slot(m, unused):
            n = (m + groups) % slots
            y = jnp.dot(normed[...], wide[n], preferred_element_type=F32)

            @pl.when(m == 1)
            def _():
                kvs[s, 1, pl.ds(first, tile), :] = y.astype(BF16)
                if ring:
                    for index in (0, 2, 1, 3):
                        ring_copy(number, index).start()

            @pl.when(m == 0)
            def _():
                kvs[s, 0, pl.ds(first, tile), :] = turned(y, n)

            @pl.when(m > 1)
            def _():
                q_all[n, pl.ds(first, tile), :] = turned(y, n)

            return unused

        lax.fori_loop(0, jnp.where(number == 0, 2, slots), one_slot, 0)
        return unused

    lax.fori_loop(0, tiles, one_tile, 0)

    if not ring:
        for step in range(1, sp):
            direct(step).start()
    group = heads // kv_heads
    q_tile = min(256, lat_rows)
    q_tiles = lat_rows // q_tile

    def block(b, unused):
        if ring:
            @pl.when(b == 0)
            def _():
                for number in range(tiles - 2):
                    forward(number)

            @pl.when(b == 1)
            def _():
                forward(tiles - 1)
                for number in range(tiles):
                    ring_wait(number, 1)

            @pl.when(b == 2)
            def _():
                for number in range(tiles):
                    ring_wait(number, 3)

            @pl.when(b == 3)
            def _():
                for number in range(tiles):
                    ring_wait(number, 4)
                    ring_wait(number, 5)

            origin = (s + jnp.where(b == 1, sp - 1, jnp.where(b == 2, 1, jnp.where(b == 3, 2, 0)))) % sp
        else:
            @pl.when(b == 1)
            def _():
                for step in range(1, sp):
                    source = lax.rem(s - step + sp, sp)
                    remote(kvs.at[source], kvs.at[source], zsend, zrecv, step - 1, "sp", source).wait_recv()

            origin = (s + b) % sp

        def q_rows(t, unused):
            if ring:
                @pl.when((b == 0) & (t == q_tiles - 1))
                def _():
                    forward(tiles - 2)

            at = pl.ds(pl.multiple_of(t * q_tile, q_tile), q_tile)
            for h in range(kv_heads):
                k = kvs[origin, 0, :, h * head : (h + 1) * head]
                v = kvs[origin, 1, :, h * head : (h + 1) * head]
                v_wide = jnp.concatenate([v, jnp.ones((keys, head), BF16)], axis=1)
                for g in range(group):
                    n = h * group + g
                    slot, lane = (n * head) // width, (n * head) % width
                    q = q_all[slot, at, lane : lane + head]
                    scores = lax.dot_general(q, k, (((1,), (1,)), ((), ())), preferred_element_type=F32)
                    scores = jnp.concatenate([scores[:, :lat_rows], scores[:, lat_rows:] + lift[n]], axis=1)
                    before = top[n, at, :]
                    now = jnp.maximum(before, jnp.max(scores, axis=-1, keepdims=True))
                    expo = jnp.exp(scores - now)
                    keep = jnp.exp(before - now)
                    top[n, at, :] = now
                    acc[n, at, :] = acc[n, at, :] * keep + jnp.dot(expo.astype(BF16), v_wide, preferred_element_type=F32)
            return unused

        lax.fori_loop(0, q_tiles, q_rows, 0)
        return unused

    lax.fori_loop(0, sp, block, 0)

    def close(t, unused):
        at = pl.ds(pl.multiple_of(t * q_tile, q_tile), q_tile)
        for pair in range(heads // 2):
            two = [acc[2 * pair + n, at, :] for n in range(2)]
            two = [v[:, :head] / v[:, head:] for v in two]
            attended[at, pair * 2 * head : (pair + 1) * 2 * head] = jnp.concatenate(two, axis=1).astype(BF16)
        return unused

    lax.fori_loop(0, q_tiles, close, 0)
    if ring:
        for number in range(tiles):
            for index in range(6):
                ring_copy(number, index).wait_send()
    else:
        for step in range(1, sp):
            direct(step).wait_send()
    for item in sends + outs:
        item.wait_send()
    gather.finish()


def back_kernel(tp, att, weight, out, full, wide, total, mixed, landed, send, recv, asend, arecv, local):
    f = lax.axis_index("tp")
    rows, cols = att.shape
    own_rows = out.shape[0]
    out_cols = weight.shape[1]
    load = pltpu.make_async_copy(weight, wide, local.at[0])
    load.start()
    mine = pltpu.make_async_copy(att, full.at[f], local.at[1])
    mine.start()
    greet(others("tp", tp))
    gather = Gather(tp, att, full, send, recv)
    gather.start()
    gather.second()
    total[...] = jnp.zeros(total.shape, F32)
    gather.relay()
    mine.wait()
    load.wait()
    r_tile = min(256, rows)

    def chip_step(index, unused):
        gather.before(index)
        chip = gather.chip(index)

        def row_step(t, unused):
            at = pl.ds(pl.multiple_of(t * r_tile, r_tile), r_tile)
            value = total[at, :]
            for n in range(2):
                source = chip * 2 + n
                depth = pl.ds(pl.multiple_of(source * cols, cols), cols)
                value = value + jnp.dot(full[source, at, :], wide[depth, :], preferred_element_type=F32)
            total[at, :] = value
            return unused

        lax.fori_loop(0, rows // r_tile, row_step, 0)
        return unused

    lax.fori_loop(0, tp // 2, chip_step, 0)
    for peer in range(tp):
        mixed[peer] = total[peer * own_rows : (peer + 1) * own_rows, :].astype(BF16)
    sends = []
    for step in range(1, tp):
        peer = lax.rem(f + step, tp)
        sends.append(remote(mixed.at[peer], landed.at[f], asend, arecv, step - 1, "tp", peer))
    for item in sends:
        item.start()
    landed[f] = mixed[f]
    for step in range(1, tp):
        origin = lax.rem(f - step + tp, tp)
        remote(landed.at[origin], landed.at[origin], asend, arecv, step - 1, "tp", origin).wait_recv()
    for n in range(tp):
        out[:, n * out_cols : (n + 1) * out_cols] = landed[n]
    for item in sends:
        item.wait_send()
    gather.finish()


def tables(first, count, head):
    freqs = head // 4
    lane = jnp.arange(2 * head, dtype=jnp.int32) % head
    inverse = 10000.0 ** (-(lane // 2 % freqs).astype(F32) / freqs)
    sign = jnp.where(lane % 2 == 0, -1.0, 1.0)
    grid_rows = -(-(count // GRID_W) // 8) * 8
    index = jnp.arange(grid_rows + GRID_W, dtype=jnp.int32)
    spot = jnp.where(index < grid_rows, index + first // GRID_W, index - grid_rows)
    angles = spot.astype(F32)[:, None] * inverse
    return jnp.cos(angles), jnp.sin(angles) * sign


def local(sp, tp, latent, context, condition, context_cond, mod_weight, norm_gain, query_weight, key_weight,
          value_weight, out_weight, query_gain, key_gain, context_lift):
    rows, model = latent.shape
    ctx_rows = context.shape[0]
    head = query_gain.shape[0]
    heads = query_weight.shape[1] // head
    kv_heads = key_weight.shape[1] // head
    width = key_weight.shape[1]
    slots = query_weight.shape[1] // width + 2
    block = rows * tp
    keys = block + ctx_rows
    limit = 60 * 1024 * 1024
    cond_pair = jax.nn.silu(jnp.stack([condition, context_cond])).astype(BF16)
    mcols = mod_weight.shape[1]
    cos, sin = tables(lax.axis_index("sp") * block, block, head)
    stacked = width % 128 != 0
    weights = [query_weight, key_weight, value_weight]
    if stacked:
        weights = [jnp.stack([query_weight[:, n * width : (n + 1) * width] for n in range(slots - 2)] + weights[1:])]
    dma = pltpu.SemaphoreType.DMA
    count = gather_sems(tp)
    pieces = (tp // 2 + 1) * 6 if sp == 4 else sp - 1
    attended, gate = pl.pallas_call(
        functools.partial(front_kernel, sp, tp, heads, kv_heads, head, stacked),
        name="front",
        out_shape=(jax.ShapeDtypeStruct((block, heads * head), BF16), jax.ShapeDtypeStruct((1, model), F32)),
        in_specs=[ANY, ANY, VMEM, ANY, VMEM, VMEM, VMEM, VMEM, VMEM, SMEM] + [ANY] * len(weights),
        out_specs=(VMEM, VMEM),
        scratch_shapes=[
            pltpu.VMEM((tp + 2, rows, model), BF16),
            pltpu.VMEM((2 * rows, model), BF16),
            pltpu.VMEM((slots, model, width), BF16),
            pltpu.VMEM(mod_weight.shape, BF16),
            pltpu.VMEM((sp, 2, mcols), F32),
            pltpu.VMEM((2, mcols), F32),
            pltpu.VMEM((2, mcols), F32),
            pltpu.VMEM((2, mcols * tp), F32),
            pltpu.VMEM((2, 1, model), F32),
            pltpu.VMEM((2, 1, model), F32),
            pltpu.VMEM((slots, 1, width), F32),
            pltpu.VMEM((slots - 2, block, width), BF16),
            pltpu.VMEM((sp, 2, keys, width), BF16),
            pltpu.VMEM((heads, block, 1), F32),
            pltpu.VMEM((heads, block, 2 * head), F32),
            dma((count,)), dma((count,)), dma((sp - 1,)), dma((sp - 1,)), dma((tp - 1,)), dma((tp - 1,)),
            dma((pieces,)), dma((pieces,)),
            dma((slots + 4,)),
        ],
        compiler_params=pltpu.CompilerParams(collective_id=0, has_side_effects=True, vmem_limit_bytes=limit),
    )(latent, context, cond_pair, mod_weight, norm_gain.reshape(1, model), cos, sin, query_gain.reshape(1, head),
      key_gain.reshape(1, head), context_lift, *weights)
    mixed = pl.pallas_call(
        functools.partial(back_kernel, tp),
        name="back",
        out_shape=jax.ShapeDtypeStruct((rows, model), BF16),
        in_specs=[VMEM, ANY],
        out_specs=VMEM,
        scratch_shapes=[
            pltpu.VMEM((tp, block, heads * head), BF16),
            pltpu.VMEM(out_weight.shape, BF16),
            pltpu.VMEM((block, out_weight.shape[1]), F32),
            pltpu.VMEM((tp, rows, out_weight.shape[1]), BF16),
            pltpu.VMEM((tp, rows, out_weight.shape[1]), BF16),
            dma((count,)), dma((count,)), dma((tp - 1,)), dma((tp - 1,)), dma((2,)),
        ],
        compiler_params=pltpu.CompilerParams(collective_id=2, has_side_effects=True, vmem_limit_bytes=limit),
    )(attended, out_weight)
    return (latent.astype(F32) + gate * mixed.astype(F32)).astype(BF16)


def solution(mesh):
    return jax.shard_map(
        functools.partial(local, mesh.shape["sp"], mesh.shape["tp"]),
        mesh=mesh,
        in_specs=(
            P(("sp", "tp"), None),
            P("sp", None),
            P("sp"),
            P("sp"),
            P("sp", "tp"),
            P(),
            P(None, "tp"),
            P(None, "tp"),
            P(None, "tp"),
            P(None, "tp"),
            P(),
            P(),
            P("tp"),
        ),
        out_specs=P(("sp", "tp"), None),
        check_vma=False,
    )
```

profile of v0, /device:TPU:0, one launch (start us, length us, event | category | flops | bytes accessed | tf_op | source)
XLA Modules:
  0.0 112.7 jit_solution(5893904971680314532)
XLA Ops:
  0.0 1.3 %fusion.1.cond = bf16[2,1024]{1,0:T(2,128)(2,1)} fusion(f32[1,1024]{1,0:T(1,128)} %bitcast.8, f32[1,1024]{1,0:T(1,128)} %bitcast.9), kind=kLoop, calls=%fused_computation.6 | loop fusion | flops 12288 | bytes 12288 | tf_op jit(solution)/shard_map/convert_element_type | solution.py:517
  1.3 0.8 fusion
  2.2 76.1 %front.1 = (bf16[512,512]{1,0:T(8,128)(2,1)}, f32[1,4096]{1,0:T(1,128)}) custom-call(bf16[64,4096]{1,0:T(8,128)(2,1)} %lat.1, bf16[128,4096]{1,0:T(8,128)(2,1)} %ctx.1, bf16[2,1024]{1,0:T(2,128)(2,1)} %fusion.1.cond, bf16[1024,1536]{1,0:T(8,128)(2,1)} %mod_weight.1, f32[1,4096]{1,0:T(1,128)} %bitcast.6, f32[72,128]{1,0:T(8,128)} %get-tuple-element.10.cos, ...), custom_call_target="tpu_custom_call" | custom-call | tf_op jit(solution)/shard_map/front/pallas_call | solution.py:527
  78.3 0.0 copy-start
  78.3 0.0 copy-start.1
  78.4 32.3 %back.1 = bf16[64,4096]{1,0:T(8,128)(2,1)} custom-call(bf16[512,512]{1,0:T(8,128)(2,1)} %get-tuple-element.8.att, bf16[4096,512]{1,0:T(8,128)(2,1)} %weight.1), custom_call_target="tpu_custom_call" | custom-call | tf_op jit(solution)/shard_map/back/pallas_call | solution.py:556
  110.7 0.0 copy-done
  110.7 0.0 copy-done.1
  110.7 2.0 %add_convert_fusion = bf16[64,4096]{1,0:T(8,128)(2,1)} fusion(bf16[64,4096]{1,0:T(8,128)(2,1)} %back.1, bf16[64,4096]{1,0:T(8,128)(2,1)S(1)} %copy-done, f32[4096]{0:T(1024)S(1)} %bitcast.7), kind=kLoop, calls=%fused_computation | loop fusion | flops 1310720 | bytes 1589248 | tf_op jit(solution)/shard_map/convert_element_type | solution.py:572
  (2 shorter events, 0.0 us)
Async XLA Ops:
  78.3 32.3 %copy-start = (bf16[64,4096]{1,0:T(8,128)(2,1)S(1)}, bf16[64,4096]{1,0:T(8,128)(2,1)}, u32[]{:S(2)}) copy-start(bf16[64,4096]{1,0:T(8,128)(2,1)} %lat.1) | copy-start | bytes 1572868
  78.3 32.3 %copy-start.1 = (f32[1,4096]{1,0:T(1,128)S(1)}, f32[1,4096]{1,0:T(1,128)}, u32[]{:S(2)}) copy-start(f32[1,4096]{1,0:T(1,128)} %get-tuple-element.7) | copy-start | bytes 49156
where the time goes:
time: 114 us; the launch traced here: 113 us
  Pallas kernels  108 us (95%)
  other arithmetic  4.17 us (4%)
    pallas_call x1, Pallas kernels, local(): pl.pallas_call(functools.partial(front_kernel, sp, tp, heads, kv_heads, h...  76.1 us
    pallas_call x1, Pallas kernels, local(): pl.pallas_call(functools.partial(back_kernel, tp), name='back', out_shape...  32.3 us

commit v1 on v0

--- a/solution.py
+++ b/solution.py
@@ -2,6 +2,7 @@
 
 import jax
 import jax.numpy as jnp
+import numpy as np
 from jax import lax
 from jax.experimental import pallas as pl
 from jax.experimental.pallas import tpu as pltpu
@@ -572,9 +573,505 @@
     return (latent.astype(F32) + gate * mixed.astype(F32)).astype(BF16)
 
 
+def partner(s, order):
+    return jnp.where(order == 0, s, jnp.where(order == 1, 3 - s, jnp.where(order == 2, (s + 2) % 4, s + 1 - 2 * (s % 2))))
+
+
+class Square:
+    def __init__(self, own, full, send, recv, base):
+        self.own, self.full, self.send, self.recv, self.base = own, full, send, recv, base
+        me = lax.axis_index("tp")
+        self.me = me
+        self.half = own.shape[0] // 2
+        core, x, y = me % 2, (me // 2) % 2, me // 4
+        self.sib = me + 1 - 2 * core
+        self.step = 1 - 2 * core
+        self.xn = me + 2 - 4 * x
+        self.yn = me + 4 - 8 * y
+        self.dn = self.xn + 4 - 8 * y
+
+    def part(self, ref, which):
+        return ref if which is None else ref.at[pl.ds(which * self.half, self.half)]
+
+    def copy(self, index):
+        me, xn, yn, dn, sib = self.me, self.xn, self.yn, self.dn, self.sib
+        origin, half, peer = {
+            0: (me, 0, xn), 1: (me, 1, xn), 2: (me, 0, yn), 3: (me, 1, yn), 4: (me, None, sib),
+            5: (xn, 1, yn), 6: (yn, 0, xn),
+            7: (xn, 0, sib), 8: (xn, 1, sib), 9: (yn, 0, sib), 10: (yn, 1, sib),
+            11: (dn, 0, sib), 12: (dn, 1, sib),
+        }[index]
+        source = self.own if index < 5 else self.full.at[origin]
+        return remote(self.part(source, half), self.part(self.full.at[origin], half), self.send, self.recv,
+                      self.base + index, "tp", peer)
+
+    def start(self, *indices):
+        for index in indices:
+            self.copy(index).start()
+
+    def arrived(self, *indices):
+        xn, yn, dn, sib, step = self.xn, self.yn, self.dn, self.sib, self.step
+        for index in indices:
+            origin, half = {
+                0: (xn, 0), 1: (xn, 1), 2: (yn, 0), 3: (yn, 1), 4: (sib, None), 5: (dn, 1), 6: (dn, 0),
+                7: (xn + step, 0), 8: (xn + step, 1), 9: (yn + step, 0), 10: (yn + step, 1),
+                11: (dn + step, 0), 12: (dn + step, 1),
+            }[index]
+            ref = self.part(self.full.at[origin], half)
+            remote(ref, ref, self.send, self.recv, self.base + index, "tp", sib).wait_recv()
+
+    def finish(self):
+        for index in range(13):
+            self.copy(index).wait_send()
+
+
+def whole_kernel(head, lat, ctx, cond, ctx_cond, mod_weight, gain, cos_in, sin_in, q_gain, k_gain, lift, wq, wk, wv, wo_in, out,
+                 full, normed, wide, mod_wide, wo, parts, partial, total_mod, mod, gsc, shf, gains, cos, sin,
+                 kv_out, kv_in, v_ones, q_out, q_in, o_out, att, total, mixed, landed, result,
+                 send, recv, psend, precv, msend, mrecv, ksend, krecv, qsend, qrecv, osend, orecv, asend, arecv,
+                 bsend, brecv, local):
+    sp, tp = 4, 8
+    s, f = lax.axis_index("sp"), lax.axis_index("tp")
+    rows, model = lat.shape
+    tile = 2 * rows
+    block = rows * tp
+    ctx_rows = ctx.shape[0]
+    mcols = partial.shape[1]
+    half_rows = rows // 2
+    width = wk.shape[1]
+    pack = 2 * head
+    chunk = block // 2
+    scale = head ** -0.5
+
+    mod_in = pltpu.make_async_copy(mod_weight, mod_wide, local.at[0])
+    mod_in.start()
+    barrier = pltpu.get_barrier_semaphore()
+    peers = others("tp", tp) + others("sp", sp)
+    for axis, peer in peers:
+        pl.semaphore_signal(barrier, inc=1, device_id={axis: peer}, device_id_type=MESH)
+    ctx_in = [pltpu.make_async_copy(ctx.at[pl.ds(n * rows, rows)], full.at[tp + n], local.at[1 + n]) for n in range(2)]
+    own = pltpu.make_async_copy(lat, full.at[f], local.at[3])
+    weights = [
+        pltpu.make_async_copy(wk, wide.at[0, :, pl.ds(0, width)], local.at[4]),
+        pltpu.make_async_copy(wv, wide.at[0, :, pl.ds(width, width)], local.at[5]),
+        pltpu.make_async_copy(wq, wide.at[1], local.at[6]),
+    ]
+    tabs = [pltpu.make_async_copy(cos_in, cos, local.at[7]), pltpu.make_async_copy(sin_in, sin, local.at[8])]
+    out_w = [pltpu.make_async_copy(wo_in.at[:, n], wo.at[n], local.at[9 + n]) for n in range(sp)]
+    pl.semaphore_wait(barrier, len(peers))
+    gather = Square(lat, full, send, recv, 0)
+    gather.start(1, 2, 4)
+    for item in ctx_in + [own] + weights + tabs + out_w:
+        item.start()
+    pair = jnp.concatenate([cond[...], ctx_cond[...]], axis=0)
+    pair = (pair / (1.0 + jnp.exp(-pair))).astype(BF16)
+    mod_in.wait()
+    first_sum = jnp.dot(pair, mod_wide[...], preferred_element_type=F32)
+    partial[...] = first_sum
+    parts[s] = first_sum
+    sends = [remote(partial, parts.at[s], psend, precv, n - 1, "sp", partner(s, n)) for n in range(1, sp)]
+    for item in sends:
+        item.start()
+    gains[0] = jnp.concatenate([k_gain[...]] * (width // head), axis=1)
+    gains[1] = jnp.concatenate([q_gain[...] * scale] * (width // head), axis=1)
+    total[...] = jnp.zeros(total.shape, F32)
+    for n in range(1, sp):
+        origin = partner(s, n)
+        remote(parts.at[origin], parts.at[origin], psend, precv, n - 1, "sp", origin).wait_recv()
+    summed = parts[0] + parts[1] + parts[2] + parts[3]
+    total_mod[...] = summed
+    here = pl.ds(pl.multiple_of(f * mcols, mcols), mcols)
+    mod[:, here] = summed
+    outs = [remote(total_mod, mod.at[:, here], msend, mrecv, step - 1, "tp", lax.rem(f + step, tp)) for step in range(1, tp)]
+    for item in outs:
+        item.start()
+    gather.start(0, 3)
+    for step in range(1, tp):
+        origin = lax.rem(f - step + tp, tp)
+        ref = mod.at[:, pl.ds(pl.multiple_of(origin * mcols, mcols), mcols)]
+        remote(ref, ref, msend, mrecv, step - 1, "tp", origin).wait_recv()
+    for r in range(2):
+        gsc[r] = gain[...] * (1.0 + mod[r : r + 1, model : 2 * model])
+        shf[r] = mod[r : r + 1, :model]
+    gather.arrived(1)
+    gather.start(5, 8)
+    gather.arrived(2)
+    gather.start(6, 9)
+    for item in ctx_in + [own] + weights + tabs:
+        item.wait()
+
+    even = lax.broadcasted_iota(jnp.int32, (tile, width), 1) % 2 == 0
+    same = (
+        lax.broadcasted_iota(jnp.int32, (width, width), 0) // head
+        == lax.broadcasted_iota(jnp.int32, (width, width), 1) // head
+    )
+    ones = jnp.where(same, 1.0, 0.0).astype(BF16)
+    by_row = (lax.broadcasted_iota(jnp.int32, (1, pack), 1) % head) // 2 < head // 4
+    low = lax.broadcasted_iota(jnp.int32, (tile, pack), 1) < head
+    grid_rows = cos.shape[0] - GRID_W
+    step_rows = 16
+    steps = half_rows // step_rows
+
+    def chip_at(index):
+        x, y = (f // 2) % 2, f // 4
+        return ((y + index // 2) % 2) * 2 + (x + index) % 2
+
+    def kv_send(number, n):
+        chip = chip_at(jnp.maximum(number - 1, 0))
+        at_out = pl.multiple_of(jnp.where(number == 0, block, chip * tile), tile)
+        at_in = pl.multiple_of(jnp.where(number == 0, sp * block + s * ctx_rows, s * block + chip * tile), tile)
+        peer = partner(s, n)
+        return remote(kv_out.at[peer, pl.ds(at_out, tile)], kv_in.at[pl.ds(at_in, tile)], ksend, krecv,
+                      number * 3 + n - 1, "sp", peer)
+
+    def kv_wait(number, n):
+        chip = chip_at(jnp.maximum(number - 1, 0))
+        origin = partner(s, n)
+        at_in = pl.multiple_of(jnp.where(number == 0, sp * block + origin * ctx_rows, origin * block + chip * tile), tile)
+        ref = kv_in.at[pl.ds(at_in, tile)]
+        remote(ref, ref, ksend, krecv, number * 3 + n - 1, "sp", origin).wait_recv()
+
+    def one_tile(number, unused):
+        @pl.when(number == 1)
+        def _():
+            gather.arrived(4)
+
+        @pl.when(number == 2)
+        def _():
+            gather.arrived(0)
+            gather.start(7)
+            gather.arrived(3)
+            gather.start(10)
+            gather.arrived(7, 8)
+
+        @pl.when(number == 3)
+        def _():
+            gather.arrived(9, 10)
+
+        @pl.when(number == 4)
+        def _():
+            gather.arrived(5)
+            gather.start(12)
+            gather.arrived(6)
+            gather.start(11)
+            gather.arrived(12, 11)
+
+        is_ctx = jnp.where(number == 0, 1, 0)
+        chip = chip_at(jnp.maximum(number - 1, 0))
+        base = jnp.where(number == 0, tp, chip * 2)
+
+        def norm_rows(j, unused):
+            slot = base + (j // steps) % 2
+            row = pl.multiple_of((j // (2 * steps)) * half_rows + (j % steps) * step_rows, step_rows)
+            v = full[slot, pl.ds(row, step_rows), :].astype(F32)
+            inv = lax.rsqrt(jnp.mean(v * v, axis=-1, keepdims=True) + EPS)
+            value = v * inv * gsc[is_ctx] + shf[is_ctx]
+            normed[pl.ds(pl.multiple_of(j * step_rows, step_rows), step_rows), :] = value.astype(BF16)
+            return unused
+
+        lax.fori_loop(0, tile // step_rows, norm_rows, 0)
+
+        def table(ref, fill):
+            pieces = []
+            for c in range(2):
+                for owner in range(2):
+                    row = ref[pl.ds(s * tp + chip * 2 + owner, 1), :]
+                    col = ref[grid_rows + c * half_rows : grid_rows + (c + 1) * half_rows, :]
+                    pieces.append(jnp.where(by_row, row, col))
+            v = jnp.concatenate(pieces, axis=0)
+            v = jnp.where(is_ctx == 1, fill, v)
+            return jnp.concatenate([v] * (width // pack), axis=1)
+
+        cos_t, sin_t = table(cos, 1.0), table(sin, 0.0)
+
+        def turned(y, row):
+            sq = y * y
+            hi = sq.astype(BF16)
+            lo = (sq - hi.astype(F32)).astype(BF16)
+            mean = jnp.dot(hi, ones, preferred_element_type=F32) + jnp.dot(lo, ones, preferred_element_type=F32)
+            u = y * lax.rsqrt(mean * (1.0 / head) + EPS) * row
+            other = jnp.where(even, pltpu.roll(u, width - 1, axis=1), pltpu.roll(u, 1, axis=1))
+            return u * cos_t + other * sin_t
+
+        y = jnp.dot(normed[...], wide[0], preferred_element_type=F32)
+        k, v = turned(y[:, :width], gains[0]), y[:, width:]
+        at_out = pl.ds(pl.multiple_of(jnp.where(number == 0, block, chip * tile), tile), tile)
+        at_in = pl.ds(pl.multiple_of(jnp.where(number == 0, sp * block + s * ctx_rows, s * block + chip * tile), tile), tile)
+        for n in range(width // pack):
+            kc, vc = k[:, n * pack : (n + 1) * pack], v[:, n * pack : (n + 1) * pack]
+            kv_out[2 * n, at_out, :] = jnp.where(low, kc, pltpu.roll(vc, head, axis=1)).astype(BF16)
+            kv_out[2 * n + 1, at_out, :] = jnp.where(low, pltpu.roll(kc, head, axis=1), vc).astype(BF16)
+        for n in range(1, sp):
+            kv_send(number, n).start()
+        kv_in[at_in, :] = kv_out[s, at_out, :]
+
+        @pl.when(number > 0)
+        def _():
+            y = jnp.dot(normed[...], wide[1], preferred_element_type=F32)
+            for n in range(2):
+                q = turned(y[:, n * width : (n + 1) * width], gains[1]).astype(BF16)
+                for m in range(2):
+                    for c in range(2):
+                        q_out[2 * n + m, c, pl.ds(pl.multiple_of(chip * rows, rows), rows), :] = (
+                            q[c * rows : (c + 1) * rows, m * pack : (m + 1) * pack])
+
+        return unused
+
+    lax.fori_loop(0, tp // 2 + 1, one_tile, 0)
+
+    def q_send(n, c):
+        peer = partner(s, n)
+        return remote(q_out.at[peer, c], q_in.at[n, c], qsend, qrecv, (n - 1) * 2 + c, "sp", peer)
+
+    for n in range(1, sp):
+        for c in range(2):
+            q_send(n, c).start()
+    q_in[0] = q_out[s]
+
+    def wait_kv(number, unused):
+        for n in range(1, sp):
+            kv_wait(number, n)
+        return unused
+
+    lax.fori_loop(0, tp // 2 + 1, wait_kv, 0)
+    keys = kv_in.shape[0]
+    v_ones[...] = jnp.concatenate([kv_in[:, head:], jnp.ones((keys, head), BF16)], axis=1)
+    for item in out_w:
+        item.wait()
+    lat_keys = sp * block
+    pieces = 2 * sp
+    lag = 2
+
+    def o_send(order, c):
+        return remote(o_out.at[order - 1, c], att.at[order, c, f], osend, orecv, (order - 1) * 2 + c, "sp", partner(s, order))
+
+    def piece_of(p):
+        order, c = p // 2, p % 2
+        return Square(att.at[order, c, f], att.at[order, c], asend, arecv, p * 13)
+
+    def back_send(c, step):
+        peer = lax.rem(f + step, tp)
+        return remote(mixed.at[c, peer], landed.at[c, f], bsend, brecv, c * (tp - 1) + step - 1, "tp", peer)
+
+    def one_step(i, unused):
+        @pl.when(i < pieces)
+        def _():
+            order, c = i // 2, i % 2
+
+            @pl.when(order > 0)
+            def _():
+                ref = q_in.at[order, c]
+                remote(ref, ref, qsend, qrecv, (order - 1) * 2 + c, "sp", partner(s, order)).wait_recv()
+
+            results = []
+            for g in range(2):
+                q = q_in[order, c, :, g * head : (g + 1) * head]
+                scores = lax.dot_general(q, kv_in[:, :head], (((1,), (1,)), ((), ())), preferred_element_type=F32)
+                scores = jnp.concatenate([scores[:, :lat_keys], scores[:, lat_keys:] + lift[2 * s + g]], axis=1)
+                peak = jnp.max(scores, axis=-1, keepdims=True)
+                expo = jnp.exp(scores - peak).astype(BF16)
+                acc = jnp.dot(expo, v_ones[...], preferred_element_type=F32)
+                results.append(acc[:, :head] / acc[:, head:])
+            value = jnp.concatenate(results, axis=1).astype(BF16)
+
+            @pl.when(order == 0)
+            def _():
+                att[0, c, f] = value
+
+            @pl.when(order > 0)
+            def _():
+                o_out[order - 1, c] = value
+                o_send(order, c).start()
+
+        def stage(delay):
+            p = i - lag - delay
+            return p, pl.when((p >= 0) & (p < pieces))
+
+        p0, guard = stage(0)
+
+        @guard
+        def _():
+            @pl.when(p0 >= 2)
+            def _():
+                order, c = p0 // 2, p0 % 2
+                ref = att.at[order, c, f]
+                remote(ref, ref, osend, orecv, (order - 1) * 2 + c, "sp", partner(s, order)).wait_recv()
+
+            piece_of(p0).start(1, 2, 4, 0, 3)
+
+        p1, guard = stage(1)
+
+        @guard
+        def _():
+            piece = piece_of(p1)
+            piece.arrived(1)
+            piece.start(5, 8)
+            piece.arrived(2)
+            piece.start(6, 9)
+            piece.arrived(0)
+            piece.start(7)
+            piece.arrived(3)
+            piece.start(10)
+
+        p2, guard = stage(2)
+
+        @guard
+        def _():
+            piece = piece_of(p2)
+            piece.arrived(5)
+            piece.start(12)
+            piece.arrived(6)
+            piece.start(11)
+
+        p3, guard = stage(3)
+
+        @guard
+        def _():
+            piece_of(p3).arrived(4, 7, 8, 9, 10, 11, 12)
+            order, c = p3 // 2, p3 % 2
+            left = jnp.concatenate([att[order, c, n] for n in range(tp)], axis=1)
+            total[c] += jnp.dot(left, wo[partner(s, order)].reshape(tp * pack, wo.shape[3]), preferred_element_type=F32)
+
+            @pl.when(order == sp - 1)
+            def _():
+                for n in range(tp):
+                    mixed[c, n] = total[c, n * half_rows : (n + 1) * half_rows, :].astype(BF16)
+                for step in range(1, tp):
+                    back_send(c, step).start()
+                landed[c, f] = mixed[c, f]
+
+        return unused
+
+    lax.fori_loop(0, pieces + lag + 3, one_step, 0)
+    cols = wo.shape[3]
+    writes = []
+    for c in range(2):
+        for step in range(1, tp):
+            origin = lax.rem(f - step + tp, tp)
+            ref = landed.at[c, origin]
+            remote(ref, ref, bsend, brecv, c * (tp - 1) + step - 1, "tp", origin).wait_recv()
+        at = slice(c * half_rows, (c + 1) * half_rows)
+        for n in range(tp):
+            there = slice(n * cols, (n + 1) * cols)
+            gate = mod[0:1, 2 * model + n * cols : 2 * model + (n + 1) * cols]
+            result[at, there] = (full[f, at, there].astype(F32) + gate * landed[c, n].astype(F32)).astype(BF16)
+        writes.append(pltpu.make_async_copy(result.at[pl.ds(c * half_rows, half_rows)], out.at[pl.ds(c * half_rows, half_rows)],
+                                            local.at[9 + sp + c]))
+        writes[-1].start()
+    for item in sends + outs:
+        item.wait_send()
+    gather.finish()
+
+    def drain_kv(number, unused):
+        for n in range(1, sp):
+            kv_send(number, n).wait_send()
+        return unused
+
+    lax.fori_loop(0, tp // 2 + 1, drain_kv, 0)
+    for n in range(1, sp):
+        for c in range(2):
+            q_send(n, c).wait_send()
+            o_send(n, c).wait_send()
+
+    def drain_pieces(p, unused):
+        piece_of(p).finish()
+        return unused
+
+    lax.fori_loop(0, pieces, drain_pieces, 0)
+    for c in range(2):
+        for step in range(1, tp):
+            back_send(c, step).wait_send()
+    for item in writes:
+        item.wait()
+
+
+def all_tables(count, head):
+    freqs = head // 4
+    lane = np.arange(2 * head) % head
+    inverse = (10000.0 ** (-(lane // 2 % freqs).astype(np.float32) / freqs)).astype(np.float32)
+    sign = np.where(lane % 2 == 0, -1.0, 1.0).astype(np.float32)
+    spot = np.concatenate([np.arange(count // GRID_W), np.arange(GRID_W)]).astype(np.float32)
+    angles = (spot[:, None] * inverse).astype(np.float32)
+    return np.cos(angles).astype(np.float32), (np.sin(angles) * sign).astype(np.float32)
+
+
+def whole(sp, tp, latent, context, condition, context_cond, mod_weight, norm_gain, query_weight, key_weight,
+          value_weight, out_weight, query_gain, key_gain, context_lift):
+    rows, model = latent.shape
+    head = query_gain.shape[0]
+    block = rows * tp
+    ctx_rows = context.shape[0]
+    width = key_weight.shape[1]
+    mcols = mod_weight.shape[1]
+    out_cols = out_weight.shape[1]
+    pack = 2 * head
+    chunk = block // 2
+    keys = sp * (block + ctx_rows)
+    cos, sin = all_tables(sp * block, head)
+    dma = lambda *shape: pltpu.SemaphoreType.DMA(shape)
+    vm = pltpu.VMEM
+    tiles = tp // 2 + 1
+    return pl.pallas_call(
+        functools.partial(whole_kernel, head),
+        name="whole",
+        out_shape=jax.ShapeDtypeStruct((rows, model), BF16),
+        in_specs=[ANY, ANY, VMEM, VMEM, ANY, VMEM, ANY, ANY, VMEM, VMEM, SMEM, ANY, ANY, ANY, ANY],
+        out_specs=ANY,
+        scratch_shapes=[
+            vm((tp + 2, rows, model), BF16),
+            vm((2 * rows, model), BF16),
+            vm((2, model, 2 * width), BF16),
+            vm(mod_weight.shape, BF16),
+            vm((sp, tp, pack, out_cols), BF16),
+            vm((sp, 2, mcols), F32),
+            vm((2, mcols), F32),
+            vm((2, mcols), F32),
+            vm((2, mcols * tp), F32),
+            vm((2, 1, model), F32),
+            vm((2, 1, model), F32),
+            vm((2, 1, width), F32),
+            vm(cos.shape, F32),
+            vm(sin.shape, F32),
+            vm((sp, block + ctx_rows, pack), BF16),
+            vm((keys, pack), BF16),
+            vm((keys, pack), BF16),
+            vm((sp, 2, chunk, pack), BF16),
+            vm((sp, 2, chunk, pack), BF16),
+            vm((sp - 1, 2, chunk, pack), BF16),
+            vm((sp, 2, tp, chunk, pack), BF16),
+            vm((2, chunk, out_cols), F32),
+            vm((2, tp, rows // 2, out_cols), BF16),
+            vm((2, tp, rows // 2, out_cols), BF16),
+            vm((rows, model), BF16),
+            dma(13), dma(13), dma(sp - 1), dma(sp - 1), dma(tp - 1), dma(tp - 1),
+            dma(tiles * 3), dma(tiles * 3), dma(6), dma(6), dma(6), dma(6),
+            dma(13 * 8), dma(13 * 8), dma(2 * (tp - 1)), dma(2 * (tp - 1)),
+            dma(9 + sp + 2),
+        ],
+        compiler_params=pltpu.CompilerParams(collective_id=1, has_side_effects=True, vmem_limit_bytes=62 * 1024 * 1024),
+    )(latent, context, condition.reshape(1, -1), context_cond.reshape(1, -1), mod_weight, norm_gain.reshape(1, model),
+      cos, sin, query_gain.reshape(1, head), key_gain.reshape(1, head), context_lift, query_weight, key_weight,
+      value_weight, out_weight.reshape(tp, sp, pack, out_cols))
+
+
+def fits(sp, tp, latent, context, key_weight, query_weight, query_gain):
+    head = query_gain.shape[0]
+    return (
+        sp == 4 and tp == 8 and latent.shape[0] == GRID_W and context.shape[0] == 2 * latent.shape[0]
+        and 2 * head == 128 and key_weight.shape[1] == sp * head and query_weight.shape[1] == 2 * sp * head
+    )
+
+
+def chosen(sp, tp, *args):
+    latent, context, query_weight, key_weight, query_gain = args[0], args[1], args[6], args[7], args[10]
+    if fits(sp, tp, latent, context, key_weight, query_weight, query_gain):
+        return whole(sp, tp, *args)
+    return local(sp, tp, *args)
+
+
 def solution(mesh):
     return jax.shard_map(
-        functools.partial(local, mesh.shape["sp"], mesh.shape["tp"]),
+        functools.partial(chosen, mesh.shape["sp"], mesh.shape["tp"]),
         mesh=mesh,
         in_specs=(
             P(("sp", "tp"), None),

time: 114 us -> 89.1 us (0.78)
  Pallas kernels: 108 us -> 87 us
  other arithmetic: 4.17 us -> 0 us
  local copies, waits for them, and re-layouts: 0.01 us -> 1.87 us
    pallas_call x2 -> x1, Pallas kernels: 108 us -> 87 us  [whole(): pl.pallas_call(functools.partial(whole_kernel, head), name='whole', out_s...]
    convert_element_type x3 -> x0, other arithmetic: 3.3 us -> none  [the longest x1 1.99 us: local(): return (latent.astype(F32) + gate * mixed.astype(F32)).astype(BF16)]
    unnamed x4 -> x1, local copies, waits for them, and re-layouts: 0.01 us -> 1.87 us
where the time goes in v1:
time: 89.1 us; the launch traced here: 88.9 us
  Pallas kernels  87 us (98%)
  local copies, waits for them, and re-layouts  1.87 us (2%)
    pallas_call x1, Pallas kernels, whole(): pl.pallas_call(functools.partial(whole_kernel, head), name='whole', out_s...  87 us
    unnamed x1, local copies, waits for them, and re-layouts  1.87 us

profile of v1, /device:TPU:0, one launch (start us, length us, event | category | flops | bytes accessed | tf_op | source)
XLA Modules:
  0.0 88.9 jit_solution(918373177431037338)
XLA Ops:
  0.0 87.0 %whole.1 = bf16[64,4096]{1,0:T(8,128)(2,1)} custom-call(bf16[64,4096]{1,0:T(8,128)(2,1)} %lat.1, bf16[128,4096]{1,0:T(8,128)(2,1)} %ctx.1, f32[1,1024]{1,0:T(1,128)} %bitcast.8, f32[1,1024]{1,0:T(1,128)} %bitcast.9, bf16[1024,1536]{1,0:T(8,128)(2,1)} %mod_weight.1, f32[1,4096]{1,0:T(1,128)} %bitcast.7, f32[96,128]{1,0:T(8,128)} %constant.4.clone.cos_in, ...), custom_call_target="tpu_custom_call" | custom-call | tf_op jit(solution)/shard_map/whole/pallas_call | solution.py:1014
  87.0 1.9 %copy.17 = bf16[64,4096]{1,0:T(8,128)(2,1)} copy(bf16[64,4096]{1,0:T(8,128)(2,1)} %whole.1) | data formatting | bytes 1048576

commit v2 on v1

--- a/solution.py
+++ b/solution.py
@@ -709,7 +709,7 @@
     by_row = (lax.broadcasted_iota(jnp.int32, (1, pack), 1) % head) // 2 < head // 4
     low = lax.broadcasted_iota(jnp.int32, (tile, pack), 1) < head
     grid_rows = cos.shape[0] - GRID_W
-    step_rows = 16
+    step_rows, wide_step = 16, 512
     steps = half_rows // step_rows
 
     def chip_at(index):
@@ -763,13 +763,21 @@
         def norm_rows(j, unused):
             slot = base + (j // steps) % 2
             row = pl.multiple_of((j // (2 * steps)) * half_rows + (j % steps) * step_rows, step_rows)
-            v = full[slot, pl.ds(row, step_rows), :].astype(F32)
-            inv = lax.rsqrt(jnp.mean(v * v, axis=-1, keepdims=True) + EPS)
-            value = v * inv * gsc[is_ctx] + shf[is_ctx]
-            normed[pl.ds(pl.multiple_of(j * step_rows, step_rows), step_rows), :] = value.astype(BF16)
+            there = pl.ds(pl.multiple_of(j * step_rows, step_rows), step_rows)
+            squares = jnp.zeros((step_rows, 128), F32)
+            for n in range(model // wide_step):
+                v = full[slot, pl.ds(row, step_rows), n * wide_step : (n + 1) * wide_step].astype(F32)
+                v = v * v
+                for m in range(wide_step // 128):
+                    squares = squares + v[:, m * 128 : (m + 1) * 128]
+            inv = lax.rsqrt(jnp.sum(squares, axis=-1, keepdims=True) * (1.0 / model) + EPS)
+            for n in range(model // wide_step):
+                cols = slice(n * wide_step, (n + 1) * wide_step)
+                v = full[slot, pl.ds(row, step_rows), cols].astype(F32)
+                normed[there, cols] = (v * inv * gsc[is_ctx, :, cols] + shf[is_ctx, :, cols]).astype(BF16)
             return unused
 
-        lax.fori_loop(0, tile // step_rows, norm_rows, 0)
+        lax.fori_loop(0, tile // step_rows, norm_rows, 0, unroll=4)
 
         def table(ref, fill):
             pieces = []
@@ -823,8 +831,8 @@
         peer = partner(s, n)
         return remote(q_out.at[peer, c], q_in.at[n, c], qsend, qrecv, (n - 1) * 2 + c, "sp", peer)
 
-    for n in range(1, sp):
-        for c in range(2):
+    for c in range(2):
+        for n in range(1, sp):
             q_send(n, c).start()
     q_in[0] = q_out[s]
 
@@ -842,107 +850,117 @@
     pieces = 2 * sp
     lag = 2
 
+    def step_at(p):
+        if isinstance(p, int):
+            return (0 if p == pieces - 1 else p if p < sp else p - sp + 1), (0 if p < sp else 1)
+        return jnp.where(p == pieces - 1, 0, jnp.where(p < sp, p, p - sp + 1)), jnp.where(p < sp, 0, 1)
+
     def o_send(order, c):
         return remote(o_out.at[order - 1, c], att.at[order, c, f], osend, orecv, (order - 1) * 2 + c, "sp", partner(s, order))
 
     def piece_of(p):
-        order, c = p // 2, p % 2
+        order, c = step_at(p)
         return Square(att.at[order, c, f], att.at[order, c], asend, arecv, p * 13)
 
     def back_send(c, step):
         peer = lax.rem(f + step, tp)
         return remote(mixed.at[c, peer], landed.at[c, f], bsend, brecv, c * (tp - 1) + step - 1, "tp", peer)
 
+    def stage_zero(p):
+        order, c = step_at(p)
+
+        def arrive():
+            ref = att.at[order, c, f]
+            remote(ref, ref, osend, orecv, (order - 1) * 2 + c, "sp", partner(s, order)).wait_recv()
+
+        if isinstance(p, int):
+            if order > 0:
+                arrive()
+        else:
+            pl.when(order > 0)(arrive)
+        piece_of(p).start(1, 2, 4, 0, 3)
+
+    def stage_one(p):
+        piece = piece_of(p)
+        piece.arrived(1)
+        piece.start(5, 8)
+        piece.arrived(2)
+        piece.start(6, 9)
+        piece.arrived(0)
+        piece.start(7)
+        piece.arrived(3)
+        piece.start(10)
+
+    def stage_two(p):
+        piece = piece_of(p)
+        piece.arrived(5)
+        piece.start(12)
+        piece.arrived(6)
+        piece.start(11)
+
+    def stage_three(p):
+        piece_of(p).arrived(4, 7, 8, 9, 10, 11, 12)
+        order, c = step_at(p)
+        left = jnp.concatenate([att[order, c, n] for n in range(tp)], axis=1)
+        total[c] += jnp.dot(left, wo[partner(s, order)].reshape(tp * pack, wo.shape[3]), preferred_element_type=F32)
+
+    def back(c):
+        for n in range(tp):
+            mixed[c, n] = total[c, n * half_rows : (n + 1) * half_rows, :].astype(BF16)
+        for step in range(1, tp):
+            back_send(c, step).start()
+        landed[c, f] = mixed[c, f]
+
     def one_step(i, unused):
-        @pl.when(i < pieces)
-        def _():
-            order, c = i // 2, i % 2
-
-            @pl.when(order > 0)
-            def _():
-                ref = q_in.at[order, c]
-                remote(ref, ref, qsend, qrecv, (order - 1) * 2 + c, "sp", partner(s, order)).wait_recv()
-
-            results = []
-            for g in range(2):
-                q = q_in[order, c, :, g * head : (g + 1) * head]
-                scores = lax.dot_general(q, kv_in[:, :head], (((1,), (1,)), ((), ())), preferred_element_type=F32)
-                scores = jnp.concatenate([scores[:, :lat_keys], scores[:, lat_keys:] + lift[2 * s + g]], axis=1)
-                peak = jnp.max(scores, axis=-1, keepdims=True)
-                expo = jnp.exp(scores - peak).astype(BF16)
-                acc = jnp.dot(expo, v_ones[...], preferred_element_type=F32)
-                results.append(acc[:, :head] / acc[:, head:])
-            value = jnp.concatenate(results, axis=1).astype(BF16)
-
-            @pl.when(order == 0)
-            def _():
-                att[0, c, f] = value
-
-            @pl.when(order > 0)
-            def _():
-                o_out[order - 1, c] = value
-                o_send(order, c).start()
-
-        def stage(delay):
+        order, c = step_at(i)
+
+        @pl.when(order > 0)
+        def _():
+            ref = q_in.at[order, c]
+            remote(ref, ref, qsend, qrecv, (order - 1) * 2 + c, "sp", partner(s, order)).wait_recv()
+
+        results = []
+        for g in range(2):
+            q = q_in[order, c, :, g * head : (g + 1) * head]
+            scores = lax.dot_general(q, kv_in[:, :head], (((1,), (1,)), ((), ())), preferred_element_type=F32)
+            scores = jnp.concatenate([scores[:, :lat_keys], scores[:, lat_keys:] + lift[2 * s + g]], axis=1)
+            peak = jnp.max(scores, axis=-1, keepdims=True)
+            expo = jnp.exp(scores - peak).astype(BF16)
+            acc = jnp.dot(expo, v_ones[...], preferred_element_type=F32)
+            results.append(acc[:, :head] / acc[:, head:])
+        value = jnp.concatenate(results, axis=1).astype(BF16)
+
+        @pl.when(order == 0)
+        def _():
+            att[0, c, f] = value
+
+        @pl.when(order > 0)
+        def _():
+            o_out[order - 1, c] = value
+            o_send(order, c).start()
+
+        for delay, stage in enumerate((stage_zero, stage_one, stage_two, stage_three)):
             p = i - lag - delay
-            return p, pl.when((p >= 0) & (p < pieces))
-
-        p0, guard = stage(0)
-
-        @guard
-        def _():
-            @pl.when(p0 >= 2)
-            def _():
-                order, c = p0 // 2, p0 % 2
-                ref = att.at[order, c, f]
-                remote(ref, ref, osend, orecv, (order - 1) * 2 + c, "sp", partner(s, order)).wait_recv()
-
-            piece_of(p0).start(1, 2, 4, 0, 3)
-
-        p1, guard = stage(1)
-
-        @guard
-        def _():
-            piece = piece_of(p1)
-            piece.arrived(1)
-            piece.start(5, 8)
-            piece.arrived(2)
-            piece.start(6, 9)
-            piece.arrived(0)
-            piece.start(7)
-            piece.arrived(3)
-            piece.start(10)
-
-        p2, guard = stage(2)
-
-        @guard
-        def _():
-            piece = piece_of(p2)
-            piece.arrived(5)
-            piece.start(12)
-            piece.arrived(6)
-            piece.start(11)
-
-        p3, guard = stage(3)
-
-        @guard
-        def _():
-            piece_of(p3).arrived(4, 7, 8, 9, 10, 11, 12)
-            order, c = p3 // 2, p3 % 2
-            left = jnp.concatenate([att[order, c, n] for n in range(tp)], axis=1)
-            total[c] += jnp.dot(left, wo[partner(s, order)].reshape(tp * pack, wo.shape[3]), preferred_element_type=F32)
-
-            @pl.when(order == sp - 1)
-            def _():
-                for n in range(tp):
-                    mixed[c, n] = total[c, n * half_rows : (n + 1) * half_rows, :].astype(BF16)
-                for step in range(1, tp):
-                    back_send(c, step).start()
-                landed[c, f] = mixed[c, f]
-
+            pl.when(p >= 0)(functools.partial(stage, p))
         return unused
 
-    lax.fori_loop(0, pieces + lag + 3, one_step, 0)
+    lax.fori_loop(0, pieces, one_step, 0)
+    stage_zero(7)
+    stage_three(3)
+    back(0)
+    stage_two(4)
+    stage_one(5)
+    stage_zero(6)
+    stage_one(7)
+    stage_three(4)
+    stage_two(5)
+    stage_one(6)
+    stage_two(7)
+    stage_three(5)
+    stage_two(6)
+    stage_three(7)
+    stage_three(6)
+    back(1)
     cols = wo.shape[3]
     writes = []
     for c in range(2):

time: 89.1 us -> 86.3 us (0.969)
  Pallas kernels: 87 us -> 84.2 us
    pallas_call x1, Pallas kernels: 87 us -> 84.2 us  [whole(): pl.pallas_call(functools.partial(whole_kernel, head), name='whole', out_s...]
where the time goes in v2:
time: 86.3 us; the launch traced here: 86.1 us
  Pallas kernels  84.2 us (98%)
  local copies, waits for them, and re-layouts  1.87 us (2%)
    pallas_call x1, Pallas kernels, whole(): pl.pallas_call(functools.partial(whole_kernel, head), name='whole', out_s...  84.2 us
    unnamed x1, local copies, waits for them, and re-layouts  1.87 us

profile of v2, /device:TPU:0, one launch (start us, length us, event | category | flops | bytes accessed | tf_op | source)
XLA Modules:
  0.0 86.1 jit_solution(3171589481380216796)
XLA Ops:
  0.0 84.2 %whole.1 = bf16[64,4096]{1,0:T(8,128)(2,1)} custom-call(bf16[64,4096]{1,0:T(8,128)(2,1)} %lat.1, bf16[128,4096]{1,0:T(8,128)(2,1)} %ctx.1, f32[1,1024]{1,0:T(1,128)} %bitcast.8, f32[1,1024]{1,0:T(1,128)} %bitcast.9, bf16[1024,1536]{1,0:T(8,128)(2,1)} %mod_weight.1, f32[1,4096]{1,0:T(1,128)} %bitcast.7, f32[96,128]{1,0:T(8,128)} %constant.4.clone.cos_in, ...), custom_call_target="tpu_custom_call" | custom-call | tf_op jit(solution)/shard_map/whole/pallas_call | solution.py:1032
  84.2 1.9 %copy.17 = bf16[64,4096]{1,0:T(8,128)(2,1)} copy(bf16[64,4096]{1,0:T(8,128)(2,1)} %whole.1) | data formatting | bytes 1048576

commit v3 on v2

--- a/solution.py
+++ b/solution.py
@@ -574,7 +574,7 @@
 
 
 def partner(s, order):
-    return jnp.where(order == 0, s, jnp.where(order == 1, 3 - s, jnp.where(order == 2, (s + 2) % 4, s + 1 - 2 * (s % 2))))
+    return jnp.where(order == 0, s, jnp.where(order == 1, s + 1 - 2 * (s % 2), jnp.where(order == 2, 3 - s, (s + 2) % 4)))
 
 
 class Square:
@@ -625,9 +625,32 @@
             self.copy(index).wait_send()
 
 
+class Cross(Square):
+    def copy(self, index):
+        origin, peer = {
+            0: (self.me, self.xn), 1: (self.me, self.yn), 2: (self.me, self.dn), 3: (self.me, self.sib),
+            4: (self.xn, self.sib), 5: (self.yn, self.sib), 6: (self.dn, self.sib),
+        }[index]
+        ref = self.full.at[origin]
+        return remote(ref, ref, self.send, self.recv, self.base + index, "tp", peer)
+
+    def arrived(self, *indices):
+        for index in indices:
+            origin = {
+                0: self.xn, 1: self.yn, 2: self.dn, 3: self.sib,
+                4: self.xn + self.step, 5: self.yn + self.step, 6: self.dn + self.step,
+            }[index]
+            ref = self.full.at[origin]
+            remote(ref, ref, self.send, self.recv, self.base + index, "tp", self.sib).wait_recv()
+
+    def finish(self):
+        for index in range(7):
+            self.copy(index).wait_send()
+
+
 def whole_kernel(head, lat, ctx, cond, ctx_cond, mod_weight, gain, cos_in, sin_in, q_gain, k_gain, lift, wq, wk, wv, wo_in, out,
                  full, normed, wide, mod_wide, wo, parts, partial, total_mod, mod, gsc, shf, gains, cos, sin,
-                 kv_out, kv_in, v_ones, q_out, q_in, o_out, att, total, mixed, landed, result,
+                 kv_out, kv_in, v_rows, q_out, q_in, o_out, att, total, mixed, landed, result, sc_a, sc_b, max_a, max_b,
                  send, recv, psend, precv, msend, mrecv, ksend, krecv, qsend, qrecv, osend, orecv, asend, arecv,
                  bsend, brecv, local):
     sp, tp = 4, 8
@@ -658,14 +681,14 @@
     ]
     tabs = [pltpu.make_async_copy(cos_in, cos, local.at[7]), pltpu.make_async_copy(sin_in, sin, local.at[8])]
     out_w = [pltpu.make_async_copy(wo_in.at[:, n], wo.at[n], local.at[9 + n]) for n in range(sp)]
+    pair = jnp.concatenate([cond[...], ctx_cond[...]], axis=0)
+    pair = (pair / (1.0 + jnp.exp(-pair))).astype(BF16)
     pl.semaphore_wait(barrier, len(peers))
     gather = Square(lat, full, send, recv, 0)
     gather.start(1, 2, 4)
+    mod_in.wait()
     for item in ctx_in + [own] + weights + tabs + out_w:
         item.start()
-    pair = jnp.concatenate([cond[...], ctx_cond[...]], axis=0)
-    pair = (pair / (1.0 + jnp.exp(-pair))).astype(BF16)
-    mod_in.wait()
     first_sum = jnp.dot(pair, mod_wide[...], preferred_element_type=F32)
     partial[...] = first_sum
     parts[s] = first_sum
@@ -716,20 +739,32 @@
         x, y = (f // 2) % 2, f // 4
         return ((y + index // 2) % 2) * 2 + (x + index) % 2
 
-    def kv_send(number, n):
+    odd = s % 2
+
+    def rows_at(number, plane):
         chip = chip_at(jnp.maximum(number - 1, 0))
-        at_out = pl.multiple_of(jnp.where(number == 0, block, chip * tile), tile)
-        at_in = pl.multiple_of(jnp.where(number == 0, sp * block + s * ctx_rows, s * block + chip * tile), tile)
-        peer = partner(s, n)
-        return remote(kv_out.at[peer, pl.ds(at_out, tile)], kv_in.at[pl.ds(at_in, tile)], ksend, krecv,
-                      number * 3 + n - 1, "sp", peer)
-
-    def kv_wait(number, n):
-        chip = chip_at(jnp.maximum(number - 1, 0))
-        origin = partner(s, n)
-        at_in = pl.multiple_of(jnp.where(number == 0, sp * block + origin * ctx_rows, origin * block + chip * tile), tile)
-        ref = kv_in.at[pl.ds(at_in, tile)]
-        remote(ref, ref, ksend, krecv, number * 3 + n - 1, "sp", origin).wait_recv()
+        at_out = jnp.where(number == 0, block, chip * tile)
+        at_in = jnp.where(number == 0, sp * block + plane * ctx_rows, plane * block + chip * tile)
+        return pl.ds(pl.multiple_of(at_out, tile), tile), pl.ds(pl.multiple_of(at_in, tile), tile)
+
+    def kv_send(number, a, n):
+        at_out, at_in = rows_at(number, s)
+        head_pack = 2 * odd + a if n == 3 else 2 * (1 - odd) + a
+        return remote(kv_out.at[head_pack, at_out], kv_in.at[a, at_in], ksend, krecv, number * 6 + a * 3 + n - 1, "sp",
+                      partner(s, n))
+
+    def kv_wait(number, a, n):
+        ref = kv_in.at[a, rows_at(number, partner(s, n))[1]]
+        remote(ref, ref, ksend, krecv, number * 6 + a * 3 + n - 1, "sp", partner(s, n)).wait_recv()
+
+    def q_copy(number, a):
+        there = pl.ds(pl.multiple_of(chip_at(number - 1) * rows, rows), rows)
+        return remote(q_out.at[2 * (1 - odd) + a, :, there], q_in.at[a, 1, :, there], qsend, qrecv, (number - 1) * 2 + a, "sp",
+                      partner(s, 1))
+
+    def q_wait(number, a):
+        ref = q_in.at[a, 1, :, pl.ds(pl.multiple_of(chip_at(number - 1) * rows, rows), rows)]
+        remote(ref, ref, qsend, qrecv, (number - 1) * 2 + a, "sp", partner(s, 1)).wait_recv()
 
     def one_tile(number, unused):
         @pl.when(number == 1)
@@ -803,15 +838,21 @@
 
         y = jnp.dot(normed[...], wide[0], preferred_element_type=F32)
         k, v = turned(y[:, :width], gains[0]), y[:, width:]
-        at_out = pl.ds(pl.multiple_of(jnp.where(number == 0, block, chip * tile), tile), tile)
-        at_in = pl.ds(pl.multiple_of(jnp.where(number == 0, sp * block + s * ctx_rows, s * block + chip * tile), tile), tile)
+        at_out, at_in = rows_at(number, s)
         for n in range(width // pack):
             kc, vc = k[:, n * pack : (n + 1) * pack], v[:, n * pack : (n + 1) * pack]
             kv_out[2 * n, at_out, :] = jnp.where(low, kc, pltpu.roll(vc, head, axis=1)).astype(BF16)
             kv_out[2 * n + 1, at_out, :] = jnp.where(low, pltpu.roll(kc, head, axis=1), vc).astype(BF16)
-        for n in range(1, sp):
-            kv_send(number, n).start()
-        kv_in[at_in, :] = kv_out[s, at_out, :]
+        for n in (2, 3, 1):
+            kv_send(number, 0, n).start()
+
+        @pl.when(number == 1)
+        def _():
+            for n in (2, 3, 1):
+                kv_send(number - 1, 1, n).start()
+
+        for a in range(2):
+            kv_in[a, at_in, :] = kv_out[2 * odd + a, at_out, :]
 
         @pl.when(number > 0)
         def _():
@@ -822,87 +863,57 @@
                     for c in range(2):
                         q_out[2 * n + m, c, pl.ds(pl.multiple_of(chip * rows, rows), rows), :] = (
                             q[c * rows : (c + 1) * rows, m * pack : (m + 1) * pack])
+            for a in range(2):
+                q_copy(number, a).start()
 
         return unused
 
     lax.fori_loop(0, tp // 2 + 1, one_tile, 0)
 
-    def q_send(n, c):
-        peer = partner(s, n)
-        return remote(q_out.at[peer, c], q_in.at[n, c], qsend, qrecv, (n - 1) * 2 + c, "sp", peer)
-
-    for c in range(2):
-        for n in range(1, sp):
-            q_send(n, c).start()
-    q_in[0] = q_out[s]
-
-    def wait_kv(number, unused):
-        for n in range(1, sp):
-            kv_wait(number, n)
+    def late_kv(number, unused):
+        for n in (2, 3, 1):
+            kv_send(number, 1, n).start()
         return unused
 
-    lax.fori_loop(0, tp // 2 + 1, wait_kv, 0)
-    keys = kv_in.shape[0]
-    v_ones[...] = jnp.concatenate([kv_in[:, head:], jnp.ones((keys, head), BF16)], axis=1)
+    lax.fori_loop(1, tp // 2 + 1, late_kv, 0)
+    for a in range(2):
+        q_in[a, 0] = q_out[2 * odd + a]
+    keys = kv_in.shape[1]
     for item in out_w:
         item.wait()
-    lat_keys = sp * block
     pieces = 2 * sp
-    lag = 2
 
     def step_at(p):
-        if isinstance(p, int):
-            return (0 if p == pieces - 1 else p if p < sp else p - sp + 1), (0 if p < sp else 1)
-        return jnp.where(p == pieces - 1, 0, jnp.where(p < sp, p, p - sp + 1)), jnp.where(p < sp, 0, 1)
-
-    def o_send(order, c):
-        return remote(o_out.at[order - 1, c], att.at[order, c, f], osend, orecv, (order - 1) * 2 + c, "sp", partner(s, order))
+        return p // 4, 1 - p % 2, (p % 4) // 2
+
+    def o_send(a, c):
+        return remote(o_out.at[a, c], att.at[a * 4 + 2 * c, f], osend, orecv, a * 2 + c, "sp", partner(s, 1))
 
     def piece_of(p):
-        order, c = step_at(p)
-        return Square(att.at[order, c, f], att.at[order, c], asend, arecv, p * 13)
+        return Cross(att.at[p, f], att.at[p], asend, arecv, p * 7)
 
     def back_send(c, step):
         peer = lax.rem(f + step, tp)
         return remote(mixed.at[c, peer], landed.at[c, f], bsend, brecv, c * (tp - 1) + step - 1, "tp", peer)
 
     def stage_zero(p):
-        order, c = step_at(p)
-
-        def arrive():
-            ref = att.at[order, c, f]
-            remote(ref, ref, osend, orecv, (order - 1) * 2 + c, "sp", partner(s, order)).wait_recv()
-
-        if isinstance(p, int):
-            if order > 0:
-                arrive()
-        else:
-            pl.when(order > 0)(arrive)
-        piece_of(p).start(1, 2, 4, 0, 3)
+        a, other, c = step_at(p)
+        if other:
+            ref = att.at[p, f]
+            remote(ref, ref, osend, orecv, a * 2 + c, "sp", partner(s, 1)).wait_recv()
+        piece_of(p).start(2, 0, 1, 3)
 
     def stage_one(p):
         piece = piece_of(p)
-        piece.arrived(1)
-        piece.start(5, 8)
-        piece.arrived(2)
-        piece.start(6, 9)
-        piece.arrived(0)
-        piece.start(7)
-        piece.arrived(3)
-        piece.start(10)
-
-    def stage_two(p):
-        piece = piece_of(p)
-        piece.arrived(5)
-        piece.start(12)
-        piece.arrived(6)
-        piece.start(11)
+        piece.arrived(0, 1, 2)
+        piece.start(4, 5, 6)
 
     def stage_three(p):
-        piece_of(p).arrived(4, 7, 8, 9, 10, 11, 12)
-        order, c = step_at(p)
-        left = jnp.concatenate([att[order, c, n] for n in range(tp)], axis=1)
-        total[c] += jnp.dot(left, wo[partner(s, order)].reshape(tp * pack, wo.shape[3]), preferred_element_type=F32)
+        piece_of(p).arrived(3, 4, 5, 6)
+        a, other, c = step_at(p)
+        source = 2 * (1 - odd) + a if other else 2 * odd + a
+        left = jnp.concatenate([att[p, n] for n in range(tp)], axis=1)
+        total[c] += jnp.dot(left, wo[source].reshape(tp * pack, wo.shape[3]), preferred_element_type=F32)
 
     def back(c):
         for n in range(tp):
@@ -911,55 +922,91 @@
             back_send(c, step).start()
         landed[c, f] = mixed[c, f]
 
-    def one_step(i, unused):
-        order, c = step_at(i)
-
-        @pl.when(order > 0)
+    key_step = block
+    first_head = lax.broadcasted_iota(jnp.int32, (1, 2 * chunk), 1) < chunk
+
+    def advance(a, m, old, old_max, new, new_max):
+        if new is not None:
+            _, other, c = step_at(m + 1)
+            if m + 1 == 0:
+                for number in range(1, tp // 2 + 1):
+                    q_wait(number, a)
+            lifts = jnp.where(first_head, lift[4 * odd + 2 * a], lift[4 * odd + 2 * a + 1])
+            q = q_in[a, other, c]
+            both = jnp.concatenate([q[:, :head], q[:, head:]], axis=0)
+            high = None
+        if old is not None:
+            peak = jnp.max(old_max[...], axis=0, keepdims=True)
+            acc = None
+        for n in range(keys // key_step):
+            there = slice(n * key_step, (n + 1) * key_step)
+            if new is not None:
+                scores = lax.dot_general(kv_in[a, there, :head], both, (((1,), (1,)), ((), ())), preferred_element_type=F32)
+                if n >= sp:
+                    scores = scores + lifts
+                new[there, :] = scores
+                part = jnp.max(scores.reshape(key_step // 8, 8, 2 * chunk), axis=0)
+                high = part if high is None else jnp.maximum(high, part)
+            if old is not None:
+                expo = jnp.exp(old[there, :] - peak).astype(BF16)
+                part = jnp.dot(v_rows[:, there], expo, preferred_element_type=F32)
+                acc = part if acc is None else acc + part
+        if new is not None:
+            new_max[...] = high
+        if old is None:
+            return
+        value = acc[:head] / acc[head : head + 1]
+        value = jnp.concatenate([value[:, :chunk], value[:, chunk:]], axis=0).T.astype(BF16)
+        _, other, c = step_at(m)
+        if other:
+            o_out[a, c] = value
+            o_send(a, c).start()
+        else:
+            att[a * 4 + m, f] = value
+
+    def run(a, m, *stages):
+        @pl.when(a == m // 4)
         def _():
-            ref = q_in.at[order, c]
-            remote(ref, ref, qsend, qrecv, (order - 1) * 2 + c, "sp", partner(s, order)).wait_recv()
-
-        results = []
-        for g in range(2):
-            q = q_in[order, c, :, g * head : (g + 1) * head]
-            scores = lax.dot_general(q, kv_in[:, :head], (((1,), (1,)), ((), ())), preferred_element_type=F32)
-            scores = jnp.concatenate([scores[:, :lat_keys], scores[:, lat_keys:] + lift[2 * s + g]], axis=1)
-            peak = jnp.max(scores, axis=-1, keepdims=True)
-            expo = jnp.exp(scores - peak).astype(BF16)
-            acc = jnp.dot(expo, v_ones[...], preferred_element_type=F32)
-            results.append(acc[:, :head] / acc[:, head:])
-        value = jnp.concatenate(results, axis=1).astype(BF16)
-
-        @pl.when(order == 0)
-        def _():
-            att[0, c, f] = value
-
-        @pl.when(order > 0)
-        def _():
-            o_out[order - 1, c] = value
-            o_send(order, c).start()
-
-        for delay, stage in enumerate((stage_zero, stage_one, stage_two, stage_three)):
-            p = i - lag - delay
-            pl.when(p >= 0)(functools.partial(stage, p))
+            for stage, p in stages:
+                stage(p)
+
+    zero, one, three = stage_zero, stage_one, stage_three
+
+    def one_head(a, unused):
+        def wait_kv(number, unused):
+            for n in range(1, sp):
+                kv_wait(number, a, n)
+            return unused
+
+        run(a, 4, (zero, 2), (one, 1))
+        lax.fori_loop(0, tp // 2 + 1, wait_kv, 0)
+        v_rows[...] = jnp.concatenate([kv_in[a, :, head:].astype(F32), jnp.ones((keys, head), F32)], axis=1).T.astype(BF16)
+        advance(a, -1, None, None, sc_a, max_a)
+        advance(a, 0, sc_a, max_a, sc_b, max_b)
+        run(a, 4, (one, 0), (one, 3), (three, 1))
+        advance(a, 1, sc_b, max_b, sc_a, max_a)
+        run(a, 1, (zero, 1))
+        run(a, 5, (zero, 5), (one, 2), (three, 0))
+        advance(a, 2, sc_a, max_a, sc_b, max_b)
+        run(a, 2, (zero, 0))
+        run(a, 6, (zero, 4), (three, 3))
+        advance(a, 3, sc_b, max_b, None, None)
+        run(a, 3, (zero, 3))
         return unused
 
-    lax.fori_loop(0, pieces, one_step, 0)
-    stage_zero(7)
-    stage_three(3)
+    lax.fori_loop(0, 2, one_head, 0)
+    zero(7)
+    one(5)
+    three(2)
+    zero(6)
+    one(4)
+    three(5)
+    three(4)
     back(0)
-    stage_two(4)
-    stage_one(5)
-    stage_zero(6)
-    stage_one(7)
-    stage_three(4)
-    stage_two(5)
-    stage_one(6)
-    stage_two(7)
-    stage_three(5)
-    stage_two(6)
-    stage_three(7)
-    stage_three(6)
+    one(7)
+    one(6)
+    three(7)
+    three(6)
     back(1)
     cols = wo.shape[3]
     writes = []
@@ -981,15 +1028,17 @@
     gather.finish()
 
     def drain_kv(number, unused):
-        for n in range(1, sp):
-            kv_send(number, n).wait_send()
+        for a in range(2):
+            for n in range(1, sp):
+                kv_send(number, a, n).wait_send()
         return unused
 
     lax.fori_loop(0, tp // 2 + 1, drain_kv, 0)
-    for n in range(1, sp):
+    for a in range(2):
         for c in range(2):
-            q_send(n, c).wait_send()
-            o_send(n, c).wait_send()
+            o_send(a, c).wait_send()
+        for number in range(1, tp // 2 + 1):
+            q_copy(number, a).wait_send()
 
     def drain_pieces(p, unused):
         piece_of(p).finish()
@@ -1051,19 +1100,23 @@
             vm(cos.shape, F32),
             vm(sin.shape, F32),
             vm((sp, block + ctx_rows, pack), BF16),
-            vm((keys, pack), BF16),
-            vm((keys, pack), BF16),
+            vm((2, keys, pack), BF16),
+            vm((pack, keys), BF16),
             vm((sp, 2, chunk, pack), BF16),
-            vm((sp, 2, chunk, pack), BF16),
-            vm((sp - 1, 2, chunk, pack), BF16),
-            vm((sp, 2, tp, chunk, pack), BF16),
+            vm((2, 2, 2, chunk, pack), BF16),
+            vm((2, 2, chunk, pack), BF16),
+            vm((2 * sp, tp, chunk, pack), BF16),
             vm((2, chunk, out_cols), F32),
             vm((2, tp, rows // 2, out_cols), BF16),
             vm((2, tp, rows // 2, out_cols), BF16),
             vm((rows, model), BF16),
+            vm((keys, 2 * chunk), F32),
+            vm((keys, 2 * chunk), F32),
+            vm((8, 2 * chunk), F32),
+            vm((8, 2 * chunk), F32),
             dma(13), dma(13), dma(sp - 1), dma(sp - 1), dma(tp - 1), dma(tp - 1),
-            dma(tiles * 3), dma(tiles * 3), dma(6), dma(6), dma(6), dma(6),
-            dma(13 * 8), dma(13 * 8), dma(2 * (tp - 1)), dma(2 * (tp - 1)),
+            dma(tiles * 6), dma(tiles * 6), dma(8), dma(8), dma(4), dma(4),
+            dma(7 * 8), dma(7 * 8), dma(2 * (tp - 1)), dma(2 * (tp - 1)),
             dma(9 + sp + 2),
         ],
         compiler_params=pltpu.CompilerParams(collective_id=1, has_side_effects=True, vmem_limit_bytes=62 * 1024 * 1024),

time: 86.3 us -> 82.3 us (0.954)
  Pallas kernels: 84.2 us -> 80.2 us
    pallas_call x1, Pallas kernels: 84.2 us -> 80.2 us  [whole(): pl.pallas_call(functools.partial(whole_kernel, head), name='whole', out_s...]
where the time goes in v3:
time: 82.3 us; the launch traced here: 82.1 us
  Pallas kernels  80.2 us (97%)
  local copies, waits for them, and re-layouts  1.87 us (2%)
    pallas_call x1, Pallas kernels, whole(): pl.pallas_call(functools.partial(whole_kernel, head), name='whole', out_s...  80.2 us
    unnamed x1, local copies, waits for them, and re-layouts  1.87 us

profile of v3, /device:TPU:0, one launch (start us, length us, event | category | flops | bytes accessed | tf_op | source)
XLA Modules:
  0.0 82.1 jit_solution(9708563765036151452)
XLA Ops:
  0.0 80.2 %whole.1 = bf16[64,4096]{1,0:T(8,128)(2,1)} custom-call(bf16[64,4096]{1,0:T(8,128)(2,1)} %lat.1, bf16[128,4096]{1,0:T(8,128)(2,1)} %ctx.1, f32[1,1024]{1,0:T(1,128)} %bitcast.8, f32[1,1024]{1,0:T(1,128)} %bitcast.9, bf16[1024,1536]{1,0:T(8,128)(2,1)} %mod_weight.1, f32[1,4096]{1,0:T(1,128)} %bitcast.7, f32[96,128]{1,0:T(8,128)} %constant.4.clone.cos_in, ...), custom_call_target="tpu_custom_call" | custom-call | tf_op jit(solution)/shard_map/whole/pallas_call | solution.py:1081
  80.2 1.9 %copy.17 = bf16[64,4096]{1,0:T(8,128)(2,1)} copy(bf16[64,4096]{1,0:T(8,128)(2,1)} %whole.1) | data formatting | bytes 1048576

commit v4 on v3

--- a/solution.py
+++ b/solution.py
@@ -648,9 +648,10 @@
             self.copy(index).wait_send()
 
 
-def whole_kernel(head, lat, ctx, cond, ctx_cond, mod_weight, gain, cos_in, sin_in, q_gain, k_gain, lift, wq, wk, wv, wo_in, out,
+def whole_kernel(head, lat, ctx, cond_in, ctx_cond_in, mod_weight, gain_in, cos_in, sin_in, q_gain_in, k_gain_in, lift_in, wq, wk, wv, wo_in, out,
                  full, normed, wide, mod_wide, wo, parts, partial, total_mod, mod, gsc, shf, gains, cos, sin,
                  kv_out, kv_in, v_rows, q_out, q_in, o_out, att, total, mixed, landed, result, sc_a, sc_b, max_a, max_b,
+                 cond, ctx_cond, gain, q_gain, k_gain, lift,
                  send, recv, psend, precv, msend, mrecv, ksend, krecv, qsend, qrecv, osend, orecv, asend, arecv,
                  bsend, brecv, local):
     sp, tp = 4, 8
@@ -668,6 +669,14 @@
 
     mod_in = pltpu.make_async_copy(mod_weight, mod_wide, local.at[0])
     mod_in.start()
+    small = [
+        pltpu.make_async_copy(src, dst, local.at[9 + 4 + 2 + n])
+        for n, (src, dst) in enumerate((
+            (cond_in, cond), (ctx_cond_in, ctx_cond), (gain_in, gain), (q_gain_in, q_gain), (k_gain_in, k_gain), (lift_in, lift),
+        ))
+    ]
+    for item in small:
+        item.start()
     barrier = pltpu.get_barrier_semaphore()
     peers = others("tp", tp) + others("sp", sp)
     for axis, peer in peers:
@@ -681,11 +690,13 @@
     ]
     tabs = [pltpu.make_async_copy(cos_in, cos, local.at[7]), pltpu.make_async_copy(sin_in, sin, local.at[8])]
     out_w = [pltpu.make_async_copy(wo_in.at[:, n], wo.at[n], local.at[9 + n]) for n in range(sp)]
-    pair = jnp.concatenate([cond[...], ctx_cond[...]], axis=0)
-    pair = (pair / (1.0 + jnp.exp(-pair))).astype(BF16)
     pl.semaphore_wait(barrier, len(peers))
     gather = Square(lat, full, send, recv, 0)
     gather.start(1, 2, 4)
+    for item in small:
+        item.wait()
+    pair = jnp.concatenate([cond[...], ctx_cond[...]], axis=0)
+    pair = (pair / (1.0 + jnp.exp(-pair))).astype(BF16)
     mod_in.wait()
     for item in ctx_in + [own] + weights + tabs + out_w:
         item.start()
@@ -884,10 +895,10 @@
     pieces = 2 * sp
 
     def step_at(p):
-        return p // 4, 1 - p % 2, (p % 4) // 2
+        return p // 4, (p % 4) // 2, p % 2
 
     def o_send(a, c):
-        return remote(o_out.at[a, c], att.at[a * 4 + 2 * c, f], osend, orecv, a * 2 + c, "sp", partner(s, 1))
+        return remote(o_out.at[a, c], att.at[a * 4 + 2 + c, f], osend, orecv, a * 2 + c, "sp", partner(s, 1))
 
     def piece_of(p):
         return Cross(att.at[p, f], att.at[p], asend, arecv, p * 7)
@@ -928,7 +939,7 @@
     def advance(a, m, old, old_max, new, new_max):
         if new is not None:
             _, other, c = step_at(m + 1)
-            if m + 1 == 0:
+            if m + 1 == 2:
                 for number in range(1, tp // 2 + 1):
                     q_wait(number, a)
             lifts = jnp.where(first_head, lift[4 * odd + 2 * a], lift[4 * odd + 2 * a + 1])
@@ -978,35 +989,35 @@
                 kv_wait(number, a, n)
             return unused
 
-        run(a, 4, (zero, 2), (one, 1))
+        run(a, 4, (one, 0), (zero, 2), (zero, 3), (one, 1))
         lax.fori_loop(0, tp // 2 + 1, wait_kv, 0)
         v_rows[...] = jnp.concatenate([kv_in[a, :, head:].astype(F32), jnp.ones((keys, head), F32)], axis=1).T.astype(BF16)
         advance(a, -1, None, None, sc_a, max_a)
         advance(a, 0, sc_a, max_a, sc_b, max_b)
-        run(a, 4, (one, 0), (one, 3), (three, 1))
+        run(a, 0, (zero, 0))
+        run(a, 4, (zero, 4), (three, 0), (three, 1))
         advance(a, 1, sc_b, max_b, sc_a, max_a)
         run(a, 1, (zero, 1))
-        run(a, 5, (zero, 5), (one, 2), (three, 0))
+        run(a, 5, (zero, 5), (one, 2))
         advance(a, 2, sc_a, max_a, sc_b, max_b)
-        run(a, 2, (zero, 0))
-        run(a, 6, (zero, 4), (three, 3))
+        run(a, 6, (three, 2))
         advance(a, 3, sc_b, max_b, None, None)
-        run(a, 3, (zero, 3))
         return unused
 
     lax.fori_loop(0, 2, one_head, 0)
+    one(3)
+    zero(6)
     zero(7)
+    three(3)
+    one(4)
     one(5)
-    three(2)
-    zero(6)
-    one(4)
+    three(4)
+    one(6)
     three(5)
-    three(4)
+    three(6)
     back(0)
     one(7)
-    one(6)
     three(7)
-    three(6)
     back(1)
     cols = wo.shape[3]
     writes = []
@@ -1082,7 +1093,7 @@
         functools.partial(whole_kernel, head),
         name="whole",
         out_shape=jax.ShapeDtypeStruct((rows, model), BF16),
-        in_specs=[ANY, ANY, VMEM, VMEM, ANY, VMEM, ANY, ANY, VMEM, VMEM, SMEM, ANY, ANY, ANY, ANY],
+        in_specs=[ANY] * 15,
         out_specs=ANY,
         scratch_shapes=[
             vm((tp + 2, rows, model), BF16),
@@ -1114,10 +1125,16 @@
             vm((keys, 2 * chunk), F32),
             vm((8, 2 * chunk), F32),
             vm((8, 2 * chunk), F32),
+            vm((1, condition.shape[0]), F32),
+            vm((1, condition.shape[0]), F32),
+            vm((1, model), F32),
+            vm((1, head), F32),
+            vm((1, head), F32),
+            pltpu.SMEM(context_lift.shape, F32),
             dma(13), dma(13), dma(sp - 1), dma(sp - 1), dma(tp - 1), dma(tp - 1),
             dma(tiles * 6), dma(tiles * 6), dma(8), dma(8), dma(4), dma(4),
             dma(7 * 8), dma(7 * 8), dma(2 * (tp - 1)), dma(2 * (tp - 1)),
-            dma(9 + sp + 2),
+            dma(9 + sp + 8),
         ],
         compiler_params=pltpu.CompilerParams(collective_id=1, has_side_effects=True, vmem_limit_bytes=62 * 1024 * 1024),
     )(latent, context, condition.reshape(1, -1), context_cond.reshape(1, -1), mod_weight, norm_gain.reshape(1, model),

time: 82.3 us -> 77.2 us (0.938)
  Pallas kernels: 80.2 us -> 75.2 us
    pallas_call x1, Pallas kernels: 80.2 us -> 75.2 us  [whole(): pl.pallas_call(functools.partial(whole_kernel, head), name='whole', out_s...]
where the time goes in v4:
time: 77.2 us; the launch traced here: 77 us
  Pallas kernels  75.2 us (97%)
  local copies, waits for them, and re-layouts  1.87 us (2%)
    pallas_call x1, Pallas kernels, whole(): pl.pallas_call(functools.partial(whole_kernel, head), name='whole', out_s...  75.2 us
    unnamed x1, local copies, waits for them, and re-layouts  1.87 us

profile of v4, /device:TPU:0, one launch (start us, length us, event | category | flops | bytes accessed | tf_op | source)
XLA Modules:
  0.0 77.0 jit_solution(15933485414831363452)
XLA Ops:
  0.0 75.2 %whole.1 = bf16[64,4096]{1,0:T(8,128)(2,1)} custom-call(bf16[64,4096]{1,0:T(8,128)(2,1)} %lat.1, bf16[128,4096]{1,0:T(8,128)(2,1)} %ctx.1, f32[1,1024]{1,0:T(1,128)} %bitcast.8, f32[1,1024]{1,0:T(1,128)} %bitcast.9, bf16[1024,1536]{1,0:T(8,128)(2,1)} %mod_weight.1, f32[1,4096]{1,0:T(1,128)} %bitcast.7, f32[96,128]{1,0:T(8,128)} %constant.4.clone.cos_in, ...), custom_call_target="tpu_custom_call" | custom-call | tf_op jit(solution)/shard_map/whole/pallas_call | solution.py:1092
  75.2 1.9 %copy.17 = bf16[64,4096]{1,0:T(8,128)(2,1)} copy(bf16[64,4096]{1,0:T(8,128)(2,1)} %whole.1) | data formatting | bytes 1048576

commit v5 on v4

--- a/solution.py
+++ b/solution.py
@@ -984,14 +984,30 @@
     zero, one, three = stage_zero, stage_one, stage_three
 
     def one_head(a, unused):
+        def wait_near(number, unused):
+            kv_wait(number, a, 1)
+            return unused
+
         def wait_kv(number, unused):
-            for n in range(1, sp):
+            for n in (2, 3):
                 kv_wait(number, a, n)
             return unused
 
+        def turn_values(there, count):
+            values = kv_in[a, there, head:].astype(F32)
+            v_rows[:, there] = jnp.concatenate([values, jnp.ones((count, head), F32)], axis=1).T.astype(BF16)
+
+        def turn_block(plane):
+            turn_values(pl.ds(pl.multiple_of(plane * block, block), block), block)
+
         run(a, 4, (one, 0), (zero, 2), (zero, 3), (one, 1))
+        lax.fori_loop(0, tp // 2 + 1, wait_near, 0)
+        turn_block(s)
+        turn_block(partner(s, 1))
         lax.fori_loop(0, tp // 2 + 1, wait_kv, 0)
-        v_rows[...] = jnp.concatenate([kv_in[a, :, head:].astype(F32), jnp.ones((keys, head), F32)], axis=1).T.astype(BF16)
+        turn_block(partner(s, 2))
+        turn_block(partner(s, 3))
+        turn_values(slice(sp * block, keys), keys - sp * block)
         advance(a, -1, None, None, sc_a, max_a)
         advance(a, 0, sc_a, max_a, sc_b, max_b)
         run(a, 0, (zero, 0))

time: 77.2 us -> 77.5 us (level)
  no operation moved by 1% of the time
where the time goes in v5:
time: 77.5 us; the launch traced here: 77.4 us
  Pallas kernels  75.5 us (97%)
  local copies, waits for them, and re-layouts  1.87 us (2%)
    pallas_call x1, Pallas kernels, whole(): pl.pallas_call(functools.partial(whole_kernel, head), name='whole', out_s...  75.5 us
    unnamed x1, local copies, waits for them, and re-layouts  1.87 us

profile of v5, /device:TPU:0, one launch (start us, length us, event | category | flops | bytes accessed | tf_op | source)
XLA Modules:
  0.0 77.4 jit_solution(9839915558588973520)
XLA Ops:
  0.0 75.5 %whole.1 = bf16[64,4096]{1,0:T(8,128)(2,1)} custom-call(bf16[64,4096]{1,0:T(8,128)(2,1)} %lat.1, bf16[128,4096]{1,0:T(8,128)(2,1)} %ctx.1, f32[1,1024]{1,0:T(1,128)} %bitcast.8, f32[1,1024]{1,0:T(1,128)} %bitcast.9, bf16[1024,1536]{1,0:T(8,128)(2,1)} %mod_weight.1, f32[1,4096]{1,0:T(1,128)} %bitcast.7, f32[96,128]{1,0:T(8,128)} %constant.4.clone.cos_in, ...), custom_call_target="tpu_custom_call" | custom-call | tf_op jit(solution)/shard_map/whole/pallas_call | solution.py:1108
  75.5 1.9 %copy.17 = bf16[64,4096]{1,0:T(8,128)(2,1)} copy(bf16[64,4096]{1,0:T(8,128)(2,1)} %whole.1) | data formatting | bytes 1048576
